TPU v7x, 256 devices: a whole 4x4x8 slice. The times are simulated.
256 devices in a mesh: sp: 64 (over z, x, core), tp: 4 (over y).
Axes of the slice: x: 4, y: 4, z: 8, core: 2. Of those that a mesh axis runs over, the one named last changes fastest.
Arguments:
- tokens: bfloat16 [16384, 2048], P(('sp', 'tp')), may hold values from -6 to 6
- norm_gain: float32 [2048], replicated, may hold values from 0.1 to 1.9
- w_glu_a: bfloat16 [2048, 2048], P(None, 'tp'), may hold values from -0.125 to 0.125
- w_glu_b: bfloat16 [2048, 2048], P(None, 'tp'), may hold values from -0.125 to 0.125
- conv_taps: float32 [31, 2048], P(None, 'tp'), may hold values from -6 to 6
- ln_gain: float32 [2048], P('tp'), may hold values from 0.1 to 1.9
- w_query: bfloat16 [2048, 2048], P(None, 'tp'), may hold values from -0.125 to 0.125
- w_key: bfloat16 [2048, 512], P(None, 'tp'), may hold values from -0.125 to 0.125
- w_value: bfloat16 [2048, 512], P(None, 'tp'), may hold values from -0.125 to 0.125
- query_gain: float32 [16, 128], P('tp'), may hold values from 1 to 40
- key_gain: float32 [4, 128], P('tp'), may hold values from 0.1 to 1.9
- lam_head: float32 [16], P('tp'), may hold values from 0.3 to 0.8
- sub_gain: float32 [128], replicated, may hold values from 0.1 to 1.9
- w_out_conv: bfloat16 [2048, 2048], P('tp'), may hold values from -0.09375 to 0.09375
- w_out_attn: bfloat16 [2048, 2048], P('tp'), may hold values from -0.09375 to 0.09375
Outputs:
- mixed: bfloat16 [16384, 2048], P(('sp', 'tp'))
- log_sums: float32 [2, 16, 16384], P(None, 'tp', 'sp')
All inputs are finite; a program needn't handle non-finite values.
Results may differ from a plain program's by a relative error of at most 0.015.
The roundings to bfloat16 on the way count: a program that leaves them out, or rounds other values in their place, can miss the bound.
Values may be sent and summed in bfloat16 or wider, within the bound.
A program may use at most 128 MiB of HBM per device.

v0:
```python
import jax
import jax.numpy as jnp
from jax import lax
from jax.sharding import PartitionSpec as P

KW = 31


def shifted(value, axis, steps):
    count = lax.axis_size(axis)
    leading, last = (max(0, -steps), min(count, count - steps))
    return lax.ppermute(value, axis, [(source, source + steps) for source in range(leading, last)])


def sent_to_all(value, axis):
    count = lax.axis_size(axis)
    return lax.all_to_all(
        jnp.broadcast_to(value[None], (count, *value.shape)), axis, 0, 0, tiled=True
    )


def taken_together(value, axis):
    everything = sent_to_all(value, axis)
    return jnp.sum(everything, axis=0)


def packed_total(arrays, axis):
    ravelled, at, outs = (jnp.concatenate([a.reshape(-1) for a in arrays]), 0, [])
    subtotal = taken_together(ravelled, axis)
    for a in arrays:
        outs.append(subtotal[at : at + a.size].reshape(a.shape))
        at += a.size
    return tuple(outs)


def sent_together(arrays, axis, dim, along):
    widths = [a.shape[along] for a in arrays]
    both = jnp.concatenate(arrays, axis=along)
    filled = lax.all_gather(both, axis, axis=dim, tiled=True)
    return tuple(jnp.split(filled, [sum(widths[:k]) for k in range(1, len(widths))], axis=along))


def cut_along(value, dim, count):
    before, after = (value.shape[:dim], value.shape[dim + 1 :])
    return jnp.moveaxis(value.reshape(*before, count, -1, *after), dim, 0)


def sum_at_owner(value, axis, dim):
    count = lax.axis_size(axis)
    blocks = lax.all_to_all(cut_along(value, dim, count), axis, 0, 0, tiled=True)
    return jnp.sum(blocks.astype(jnp.float32), axis=0)


def rms_scale(inputs_arr, gain_vec, epsilon):
    return (
        inputs_arr
        * lax.rsqrt(jnp.mean(inputs_arr * inputs_arr, axis=-1, keepdims=True) + epsilon)
        * gain_vec
    )


def attend_rows(totals, key_rows, value_rows, key_start, query_start, queries, kv_local):
    row_count = key_rows.shape[0]
    head_dim = queries.shape[4]
    key_grid = key_rows.reshape(row_count, kv_local, 2, head_dim)
    value_grid = value_rows.reshape(row_count, kv_local, -1)
    run_max, run_sum, run_acc = totals
    scores = jnp.einsum(
        "tkgmd,rkmd->kgmtr", queries, key_grid, preferred_element_type=jnp.float32
    ) * head_dim ** (-0.5)
    query_pos = query_start + jnp.arange(queries.shape[0], dtype=jnp.int32)
    key_pos = key_start + jnp.arange(row_count, dtype=jnp.int32)
    visible = (key_pos[None, :] <= query_pos[:, None]) & (key_pos[None, :] >= 0)
    scores = jnp.where(visible, scores, -1e30)
    new_max = jnp.maximum(run_max, jnp.max(scores, axis=-1))
    rescale = jnp.exp(run_max - new_max)
    weights = jnp.where(visible, jnp.exp(scores - new_max[..., None]), 0.0)
    new_sum = run_sum * rescale + jnp.sum(weights, axis=-1)
    contrib = jnp.einsum(
        "kgmtr,rkv->kgmtv",
        weights.astype(jnp.bfloat16),
        value_grid,
        preferred_element_type=jnp.float32,
    )
    new_acc = run_acc * rescale[..., None] + contrib
    return (new_max, new_sum, new_acc)


def attend_span(totals, key_rows, value_rows, query_start, queries, kv_local, shard_rows):
    total_rows = key_rows.shape[0]
    shard_count = total_rows // shard_rows
    per_step = 1
    for candidate in range(1, shard_count + 1):
        if shard_count % candidate == 0 and candidate * shard_rows <= 1024:
            per_step = candidate
    step_rows = per_step * shard_rows
    step_count = shard_count // per_step
    key_blocks = key_rows.reshape(step_count, step_rows, key_rows.shape[1])
    value_blocks = value_rows.reshape(step_count, step_rows, value_rows.shape[1])

    def one_step(running, inputs):
        key_blk, value_blk, blk_idx = inputs
        return (
            attend_rows(
                running, key_blk, value_blk, blk_idx * step_rows, query_start, queries, kv_local
            ),
            None,
        )

    final_state, unused = lax.scan(
        one_step, totals, (key_blocks, value_blocks, jnp.arange(step_count, dtype=jnp.int32))
    )
    return final_state


def empty_state(kv_local, group_size, row_count, value_dim):
    return (
        jnp.full((kv_local, group_size, 2, row_count), -1e30, jnp.float32),
        jnp.zeros((kv_local, group_size, 2, row_count), jnp.float32),
        jnp.zeros((kv_local, group_size, 2, row_count, value_dim), jnp.float32),
    )


def finish_heads(totals, lam_head, sub_gain, kv_local, group_size):
    run_max, run_sum, run_acc = totals
    row_count = run_max.shape[3]
    mixed_maps = run_acc / run_sum[..., None]
    lam_grid = lam_head.reshape(kv_local, group_size)[:, :, None, None]
    diff_out = mixed_maps[:, :, 0] - lam_grid * mixed_maps[:, :, 1]
    head_out = rms_scale(diff_out, sub_gain, 1e-06).astype(jnp.bfloat16)
    attn_rows = head_out.transpose(2, 0, 1, 3).reshape(row_count, -1)
    log_rows = (
        (run_max + jnp.log(run_sum)).reshape(kv_local * group_size, 2, row_count).transpose(1, 0, 2)
    )
    return (attn_rows, log_rows)


def on_device(
    tokens,
    norm_gain,
    w_glu_a,
    w_glu_b,
    conv_taps,
    ln_gain,
    w_query,
    w_key,
    w_value,
    query_gain,
    key_gain,
    lam_head,
    sub_gain,
    w_out_conv,
    w_out_attn,
):
    tp_count = lax.axis_size("tp")
    tok_dev = tokens.shape[0] * tp_count
    seq_offset = lax.axis_index("sp") * tok_dev
    conv_local = w_glu_a.shape[1]
    head_local = lam_head.shape[0]
    kv_local = key_gain.shape[0]
    head_dim = key_gain.shape[1] // 2
    query_cols = w_query.shape[1]
    key_cols = w_key.shape[1]
    normed = rms_scale(tokens.astype(jnp.float32), norm_gain, 1e-06).astype(jnp.bfloat16)
    rows_block = lax.all_gather(normed, "tp", axis=0, tiled=True)
    glu_a = jnp.dot(rows_block, w_glu_a, preferred_element_type=jnp.float32)
    glu_b = jnp.dot(rows_block, w_glu_b, preferred_element_type=jnp.float32)
    gated_part = (glu_a * jax.nn.sigmoid(glu_b)).astype(jnp.bfloat16)
    query_part = jnp.dot(rows_block, w_query, preferred_element_type=jnp.float32).reshape(
        -1, head_local, 2, head_dim
    )
    query_part = (
        rms_scale(query_part, query_gain.reshape(head_local, 2, head_dim), 1e-06)
        .astype(jnp.bfloat16)
        .reshape(-1, query_cols)
    )
    key_part = jnp.dot(rows_block, w_key, preferred_element_type=jnp.float32).reshape(
        -1, kv_local, 2, head_dim
    )
    key_part = (
        rms_scale(key_part, key_gain.reshape(kv_local, 2, head_dim), 1e-06)
        .astype(jnp.bfloat16)
        .reshape(-1, key_cols)
    )
    value_part = jnp.dot(rows_block, w_value, preferred_element_type=jnp.float32).astype(
        jnp.bfloat16
    )
    projected = jnp.concatenate([gated_part, query_part, key_part, value_part], axis=1)
    group_size = head_local // kv_local
    gated_rows = projected[:, :conv_local]
    queries = projected[:, conv_local : conv_local + query_cols].reshape(
        tok_dev, kv_local, group_size, 2, head_dim
    )
    key_rows = projected[:, conv_local + query_cols : conv_local + query_cols + key_cols]
    value_rows = projected[:, conv_local + query_cols + key_cols :]
    value_dim = value_rows.shape[1] // kv_local
    prev_rows = shifted(gated_rows[tok_dev - (KW - 1) :], "sp", 1)
    padded = jnp.concatenate([prev_rows, gated_rows], axis=0)
    conv_sum = jnp.zeros((tok_dev, conv_local), jnp.float32)
    for tap_idx in range(KW):
        conv_sum = conv_sum + conv_taps[tap_idx] * padded[tap_idx : tap_idx + tok_dev].astype(
            jnp.float32
        )
    chan_total = conv_local * tp_count
    sum_one, sum_two = packed_total(
        (jnp.sum(conv_sum, axis=1), jnp.sum(conv_sum * conv_sum, axis=1)), "tp"
    )
    mean_val = (sum_one / chan_total)[:, None]
    mean_sq = (sum_two / chan_total)[:, None]
    conv_out = jax.nn.silu(
        (conv_sum - mean_val) * lax.rsqrt(mean_sq - mean_val * mean_val + 1e-05) * ln_gain
    ).astype(jnp.bfloat16)
    start_state = empty_state(kv_local, group_size, tok_dev, value_dim)
    pieces = sent_together((key_rows, value_rows), "sp", 0, 1)
    totals = lax.cond(
        jnp.int32(0) <= seq_offset + tok_dev - 1,
        lambda running: attend_span(
            running, pieces[0], pieces[1], seq_offset, queries, kv_local, tok_dev
        ),
        lambda running: running,
        start_state,
    )
    attn_out, log_sums = finish_heads(totals, lam_head, sub_gain, kv_local, group_size)
    out_part = jnp.dot(conv_out, w_out_conv, preferred_element_type=jnp.float32)
    out_part = out_part + jnp.dot(attn_out, w_out_attn, preferred_element_type=jnp.float32)
    mixed = sum_at_owner(
        lax.optimization_barrier(out_part.astype(jnp.bfloat16))
        .astype(jnp.float32)
        .astype(jnp.bfloat16),
        "tp",
        0,
    )
    return (mixed.astype(jnp.bfloat16), log_sums)


def solution(mesh):
    return jax.shard_map(
        on_device,
        mesh=mesh,
        in_specs=(
            P(("sp", "tp"), None),
            P(),
            P(None, "tp"),
            P(None, "tp"),
            P(None, "tp"),
            P("tp"),
            P(None, "tp"),
            P(None, "tp"),
            P(None, "tp"),
            P("tp", None),
            P("tp", None),
            P("tp"),
            P(),
            P("tp", None),
            P("tp", None),
        ),
        out_specs=(P(("sp", "tp"), None), P(None, "tp", "sp")),
        check_vma=False,
    )
```

profile of v0, /device:TPU:64, one launch (start us, length us, event | category | flops | bytes accessed | tf_op | source)
XLA Modules:
  0.0 380.5 jit_solution(15534507754161818594)
XLA Ops:
  10.4 29.0 %all-gather.3.cloned.1.call-done = bf16[256,2048]{1,0:T(8,128)(2,1)} async-done(((bf16[64,2048]{1,0:T(8,128)(2,1)}), bf16[256,2048]{1,0:T(8,128)(2,1)}) %all-gather.3.cloned.1.call-update) | async-done | bytes 1048592 | tf_op jit(solution)/shard_map/all_gather | solution.py:165
  45.4 3.4 fusion.69
  50.8 2.5 fusion.21
  57.3 4.1 %collective-permute-done = bf16[30,512]{1,0:T(8,128)(2,1)S(1)} collective-permute-done((bf16[30,512]{1,0:T(8,128)(2,1)S(1)}, bf16[30,512]{1,0:T(8,128)(2,1)S(1)}, u32[]{:S(2)}, u32[]{:S(2)}) %collective-permute-start) | collective-permute-done | bytes 30752 | tf_op jit(solution)/shard_map/ppermute | solution.py:12
  61.4 3.5 fusion.65
  65.5 3.4 all-to-all-start
  69.0 5.1 %all-to-all-done = f32[4,1,512]{2,1,0:T(1,128)S(1)} async-done(((f32[4,1,512]{2,1,0:T(1,128)}), f32[4,1,512]{2,1,0:T(1,128)S(1)}, u32[]{:S(2)}, u32[]{:S(2)}) %all-to-all-start) | async-done | bytes 8224 | tf_op jit(solution)/shard_map/all_to_all | solution.py:17
  74.2 2.9 fusion.28
  77.1 52.1 %all-gather.5.cloned.1.call-done = bf16[16384,256]{0,1:T(8,128)(2,1)} async-done(((bf16[256,256]{0,1:T(8,128)(2,1)}), bf16[16384,256]{0,1:T(8,128)(2,1)}) %all-gather.5.cloned.1.call-update) | async-done | bytes 8388624 | tf_op jit(solution)/shard_map/all_gather | solution.py:39
  129.1 219.6 %conditional.1 = (f32[1,4,2,256]{3,1,2,0:T(4,128)}, f32[1,4,2,256]{3,1,2,0:T(4,128)}, f32[1,4,2,256,128]{3,4,1,2,0:T(8,128)}, f32[1,4,2,256]{3,1,2,0:T(4,128)S(1)}) conditional(s32[]{:T(128)} %convert_element_type.183, () %tuple.20, (bf16[16384,256]{0,1:T(8,128)(2,1)}, s32[]{:T(128)}, bf16[256,1,4,2,64]{0,4,3,2,1:T(8,128)(2,1)S(1)}) %tuple.21), branch_computations={%region_6.7_spmd, %region_7.12_spmd} | conditional | flops 825507072 | bytes 74617264 | solution.py:215
  129.2 11.9 %copy.46 = bf16[16384,256]{1,0:T(8,128)(2,1)} copy(bf16[16384,256]{0,1:T(8,128)(2,1)} %get-tuple-element.135) | data formatting | bytes 16777216 | tf_op jit(solution)/shard_map
  141.1 5.7 %fusion.66 = (bf16[16384,128]{1,0:T(8,128)(2,1)}, bf16[16384,128]{1,0:T(8,128)(2,1)}) fusion(bf16[16384,256]{1,0:T(8,128)(2,1)} %copy.46), kind=kLoop, calls=%fused_computation.139 | loop fusion | bytes 16777216 | tf_op jit(solution)/shard_map/split | solution.py:40
  146.8 198.6 %while.14 = (s32[]{:T(128)}, f32[1,4,2,256]{3,1,2,0:T(4,128)}, f32[1,4,2,256]{3,1,2,0:T(4,128)}, f32[1,4,2,256,128]{4,3,2,1,0:T(8,128)}, s32[16]{0:T(128)S(1)}, ...) while((s32[]{:T(128)}, f32[1,4,2,256]{3,1,2,0:T(4,128)}, ...), condition=%wide.region_11.11_spmd.clone, body=%wide.region_8.10_spmd.clone.sunk | while | flops 825507072 | bytes 38424812 | solution.py:110
  151.1 2.3 fusion.96
  154.0 2.9 fusion.97
  162.9 2.3 fusion.96
  166.5 2.9 fusion.97
  175.4 2.3 fusion.96
  179.0 2.9 fusion.97
  187.9 2.3 fusion.96
  191.5 2.9 fusion.97
  200.4 2.3 fusion.96
  204.0 2.9 fusion.97
  212.8 2.3 fusion.96
  216.5 2.9 fusion.97
  225.3 2.3 fusion.96
  229.0 2.9 fusion.97
  237.8 2.3 fusion.96
  241.5 2.9 fusion.97
  250.3 2.3 fusion.96
  254.0 2.9 fusion.97
  262.8 2.3 fusion.96
  266.5 2.9 fusion.97
  275.3 2.3 fusion.96
  279.0 2.9 fusion.97
  287.8 2.3 fusion.96
  291.5 2.9 fusion.97
  300.3 2.3 fusion.96
  304.0 2.9 fusion.97
  312.8 2.3 fusion.96
  316.5 2.9 fusion.97
  325.3 2.3 fusion.96
  329.0 2.9 fusion.97
  337.8 2.3 fusion.96
  341.5 2.9 fusion.97
  345.4 2.6 copy.54
  353.0 4.3 %all-to-all-start.1 = ((bf16[4,64,2048]{2,1,0:T(8,128)(2,1)}), bf16[4,64,2048]{2,1,0:T(8,128)(2,1)S(1)}, u32[]{:S(2)}, u32[]{:S(2)}) async-start(bf16[4,64,2048]{2,1,0:T(8,128)(2,1)} %bitcast.158), calls=%async_computation.1 | async-start | bytes 2097152 | tf_op jit(solution)/shard_map/all_to_all | solution.py:50
  358.6 14.2 %all-to-all-done.1 = bf16[4,64,2048]{2,1,0:T(8,128)(2,1)S(1)} async-done(((bf16[4,64,2048]{2,1,0:T(8,128)(2,1)}), bf16[4,64,2048]{2,1,0:T(8,128)(2,1)S(1)}, u32[]{:S(2)}, u32[]{:S(2)}) %all-to-all-start.1) | async-done | bytes 1048608 | tf_op jit(solution)/shard_map/all_to_all | solution.py:50
  (316 shorter events, 125.8 us)
Async XLA Ops:
  7.2 67.0 %copy-start = (bf16[512,2048]{1,0:T(8,128)(2,1)S(1)}, bf16[512,2048]{1,0:T(8,128)(2,1)}, u32[]{:S(2)}) copy-start(bf16[512,2048]{1,0:T(8,128)(2,1)} %param.32) | copy-start | bytes 6291460
  7.2 37.5 %copy-start.10 = (f32[4,128]{1,0:T(4,128)S(1)}, f32[4,128]{1,0:T(4,128)}, u32[]{:S(2)}) copy-start(f32[4,128]{1,0:T(4,128)} %param.28) | copy-start | bytes 6148
  7.2 37.6 %copy-start.8 = (f32[31,512]{1,0:T(8,128)S(1)}, f32[31,512]{1,0:T(8,128)}, u32[]{:S(2)}) copy-start(f32[31,512]{1,0:T(8,128)} %param.23) | copy-start | bytes 190468
  7.2 32.2 %all-gather.3.cloned.1.call-start = ((), (), s32[]{:S(2)}) async-start(), calls=%async_computation.2 | async-start | bytes 1310720 | tf_op jit(solution)/shard_map/all_gather | solution.py:165
  10.3 118.8 %all-gather.5.cloned.1.call-start = ((), (), s32[]{:S(2)}) async-start(), calls=%async_computation.3 | async-start | bytes 8519680 | tf_op jit(solution)/shard_map/all_gather | solution.py:39
  39.4 6.0 %copy-start.1 = (bf16[256,2048]{1,0:T(8,128)(2,1)S(1)}, bf16[256,2048]{1,0:T(8,128)(2,1)}, u32[]{:S(2)}) copy-start(bf16[256,2048]{1,0:T(8,128)(2,1)} %all-gather.3.cloned.1.call-done) | copy-start | bytes 3145732
  50.8 2.5 copy-start.5
  50.8 5.2 %copy-start.4 = (f32[256,512]{0,1:T(8,128)S(1)}, f32[256,512]{0,1:T(8,128)}, u32[]{:S(2)}) copy-start(f32[256,512]{0,1:T(8,128)} %copy.45) | copy-start | bytes 1572868
  54.0 7.3 %collective-permute-start = (bf16[30,512]{1,0:T(8,128)(2,1)S(1)}, bf16[30,512]{1,0:T(8,128)(2,1)S(1)}, u32[]{:S(2)}, u32[]{:S(2)}) collective-permute-start(bf16[30,512]{1,0:T(8,128)(2,1)S(1)} %slice.264), channel_id=1, source_target_pairs={{0,4},{4,8},{8,12},{12,16},{16,20},{20,24},{24,28},{28,32},{32,36}... | collective-permute-start | bytes 92168 | tf_op jit(solution)/shard_map/ppermute | solution.py:12
  65.5 8.7 %all-to-all-start = ((f32[4,1,512]{2,1,0:T(1,128)}), f32[4,1,512]{2,1,0:T(1,128)S(1)}, u32[]{:S(2)}, u32[]{:S(2)}) async-start(f32[4,1,512]{2,1,0:T(1,128)} %broadcast_in_dim.37), calls=%async_computation | async-start | bytes 16384 | tf_op jit(solution)/shard_map/all_to_all | solution.py:17
  129.1 221.1 %copy-start.9 = (f32[4]{0:T(128)S(1)}, f32[4]{0:T(128)}, u32[]{:S(2)}) copy-start(f32[4]{0:T(128)} %param.30) | copy-start | bytes 52
  129.1 221.3 %copy-start.11 = (f32[128]{0:T(128)S(1)}, f32[128]{0:T(128)}, u32[]{:S(2)}) copy-start(f32[128]{0:T(128)} %param.31) | copy-start | bytes 1540
  151.1 3.0 copy-start.6
  157.0 1.0 copy-start.7
  162.8 3.7 copy-start.6
  169.5 1.0 copy-start.7
  175.3 3.7 copy-start.6
  182.0 1.0 copy-start.7
  187.8 3.7 copy-start.6
  194.5 1.0 copy-start.7
  200.3 3.7 copy-start.6
  207.0 1.0 copy-start.7
  212.8 3.7 copy-start.6
  219.5 1.0 copy-start.7
  225.3 3.7 copy-start.6
  232.0 1.0 copy-start.7
  237.8 3.7 copy-start.6
  244.5 1.0 copy-start.7
  250.3 3.7 copy-start.6
  257.0 1.0 copy-start.7
  262.8 3.7 copy-start.6
  269.4 1.0 copy-start.7
  275.3 3.7 copy-start.6
  281.9 1.0 copy-start.7
  287.8 3.7 copy-start.6
  294.4 1.0 copy-start.7
  300.3 3.7 copy-start.6
  306.9 1.0 copy-start.7
  312.8 3.7 copy-start.6
  319.4 1.0 copy-start.7
  325.3 3.7 copy-start.6
  331.9 1.0 copy-start.7
  337.8 3.7 copy-start.6
  344.4 1.0 copy-start.7
  348.7 1.9 copy-start.2
  348.7 2.6 copy-start.3
  353.0 19.8 %all-to-all-start.1 = ((bf16[4,64,2048]{2,1,0:T(8,128)(2,1)}), bf16[4,64,2048]{2,1,0:T(8,128)(2,1)S(1)}, u32[]{:S(2)}, u32[]{:S(2)}) async-start(bf16[4,64,2048]{2,1,0:T(8,128)(2,1)} %bitcast.158), calls=%async_computation.1 | async-start | bytes 2097152 | tf_op jit(solution)/shard_map/all_to_all | solution.py:50
Sparse Core Ops, SparseCore 0:
  10.4 28.9 all-gather.2
  44.8 84.3 all-gather.4
where the time goes:
time: 387 us; the launch traced here: 381 us
  waiting for transfers between devices  104 us (27%)
  other arithmetic  86.7 us (22%)
  matrix products  84.3 us (22%)
  local copies, waits for them, and re-layouts  69.5 us (18%)
  between operations  14.3 us (4%)
  loops' own time  11.6 us (3%)
  starting transfers between devices  9.71 us (3%)
    all_gather x1, waiting for transfers between devices, sent_together(): filled = lax.all_gather(both, axis, axis=dim, tiled=True)  52.1 us
    dot_general x16, matrix products, attend_rows(): jnp.einsum('kgmtr,rkv->kgmtv', weights.astype(jnp.bfloat16), value_grid,...  46.7 us
    another operation x16, other arithmetic  37.4 us
    all_gather x1, waiting for transfers between devices, on_device(): rows_block = lax.all_gather(normed, 'tp', axis=0, tiled=True)  29 us
    dynamic_slice x48, local copies, waits for them, and re-layouts, attend_span(): lax.scan(one_step, totals, (key_blocks, value_blocks, jnp.arange(step_cou...  27.6 us
    dot_general x16, matrix products, attend_rows(): jnp.einsum('tkgmd,rkmd->kgmtr', queries, key_grid, preferred_element_type...  22.6 us
    add x16, other arithmetic, attend_rows(): new_sum = run_sum * rescale + jnp.sum(weights, axis=-1)  20.7 us
    while x80, local copies, waits for them, and re-layouts  15.5 us
  transfers between devices with their start and end apart: 5, of which 5 were waited for; matrix products, arithmetic and copies ran while one was open for 5% of the time, Pallas kernels for 0%

commit v1 on v0

v1 whole, which is shorter than its diff:
```python
import functools

import jax
import jax.numpy as jnp
from jax import lax
from jax.experimental import pallas as pl
from jax.experimental.pallas import tpu as pltpu
from jax.sharding import PartitionSpec as P

KW = 31
MESH = pl.DeviceIdType.MESH
NZ, NX, NT = 8, 4, 4
BF, F32 = jnp.bfloat16, jnp.float32
VM = pl.BlockSpec(memory_space=pltpu.VMEM)
ANY = pl.BlockSpec(memory_space=pl.ANY)


def remote(src, dst, send, recv, device):
    return pltpu.make_async_remote_copy(
        src_ref=src, dst_ref=dst, send_sem=send, recv_sem=recv, device_id=device, device_id_type=MESH
    )


def greet(devices):
    barrier = pltpu.get_barrier_semaphore()
    for device in devices:
        pl.semaphore_signal(barrier, inc=1, device_id=device, device_id_type=MESH)
    return lambda: pl.semaphore_wait(barrier, len(devices))


def half_norm(value, gain):
    low = lax.broadcasted_iota(jnp.int32, value.shape, 1) < 64
    squares = value * value
    first = jnp.sum(jnp.where(low, squares, 0.0), axis=1, keepdims=True)
    second = jnp.sum(jnp.where(low, 0.0, squares), axis=1, keepdims=True)
    scale = jnp.where(low, lax.rsqrt(first / 64 + 1e-6), lax.rsqrt(second / 64 + 1e-6))
    return (value * scale * gain).astype(BF)


def front_kernel(
    tok, gain, wa_h, wb_h, wq_h, wk_h, wv_h, qg, kg,
    gated, q_own, q_far, kv,
    rows, normed, wa, wb, wq, wk, wv, w_sem, own_sem, s1, r1, s2, r2,
):
    y = lax.axis_index("tp")
    up, down = lax.rem(y + 1, NT), lax.rem(y + 3, NT)
    meet = greet([{"tp": up}, {"tp": down}])
    loads = [
        pltpu.make_async_copy(src, dst, w_sem.at[i])
        for i, (src, dst) in enumerate(((wa_h, wa), (wb_h, wb), (wq_h, wq), (wk_h, wk), (wv_h, wv)))
    ]
    own = pltpu.make_async_copy(tok, rows.at[y], own_sem)
    own.start()
    meet()
    sends = []

    def piece(slot, half):
        return rows.at[slot, pl.ds(half * 32, 32)]

    for order in range(2):
        for d, target in enumerate((up, down)):
            half = order if d == 0 else 1 - order
            copy = remote(tok.at[pl.ds(half * 32, 32)], piece(y, half), s1.at[d, half], r1.at[d, half], {"tp": target})
            copy.start()
            sends.append(copy)
    for load in loads:
        load.start()
    own.wait()

    def norm_slot(slot):
        value = rows[slot].astype(F32)
        scale = lax.rsqrt(jnp.mean(value * value, axis=1, keepdims=True) + 1e-6)
        normed[pl.ds(pl.multiple_of(slot * 64, 64), 64), :] = (value * scale * gain[...]).astype(BF)

    norm_slot(y)
    for d, (target, source) in enumerate(((up, down), (down, up))):
        half = d
        remote(piece(source, half), piece(source, half), s1.at[d, half], r1.at[d, half], {"tp": target}).wait_recv()
        copy = remote(piece(source, half), piece(source, half), s2.at[d], r2.at[d], {"tp": target})
        copy.start()
        sends.append(copy)
    for d, (target, source) in enumerate(((up, down), (down, up))):
        half = 1 - d
        remote(piece(source, half), piece(source, half), s1.at[d, half], r1.at[d, half], {"tp": target}).wait_recv()
        norm_slot(source)
    far = lax.rem(y + 2, NT)
    for d, target in enumerate((up, down)):
        remote(piece(far, d), piece(far, d), s2.at[d], r2.at[d], {"tp": target}).wait_recv()
    norm_slot(far)
    for load in loads:
        load.wait()
    value = normed[...]

    def dot(weight):
        return jnp.dot(value, weight, preferred_element_type=F32)

    key_value = dot(jnp.concatenate([wk[...], wv[...]], axis=1))
    keys = half_norm(key_value[:, :128], kg[...])
    for h in range(2):
        kv[h, :, 0:128] = keys[h * 128 : (h + 1) * 128].T
        kv[h, :, 128:256] = key_value[h * 128 : (h + 1) * 128, 128:].astype(BF)
    for n in range(2):
        span = slice(n * 256, (n + 1) * 256)
        queries = dot(wq[:, span])
        target = q_own if n == 0 else q_far
        for k in range(2):
            part = half_norm(queries[:, k * 128 : (k + 1) * 128], qg[2 * n + k : 2 * n + k + 1, :])
            target[:, k * 128 : (k + 1) * 128] = part * jnp.asarray(0.125, BF)
    for n in range(2):
        span = slice(n * 256, (n + 1) * 256)
        gated[:, span] = (dot(wa[:, span]) * jax.nn.sigmoid(dot(wb[:, span]))).astype(BF)
    for copy in sends:
        copy.wait_send()


def front(tokens, norm_gain, wa, wb, wq, wk, wv, query_gain, key_gain):
    dma = pltpu.SemaphoreType.DMA
    return pl.pallas_call(
        front_kernel,
        out_shape=(
            jax.ShapeDtypeStruct((256, 512), BF),
            jax.ShapeDtypeStruct((256, 256), BF),
            jax.ShapeDtypeStruct((256, 256), BF),
            jax.ShapeDtypeStruct((2, 128, 256), BF),
        ),
        in_specs=[VM, VM, ANY, ANY, ANY, ANY, ANY, VM, VM],
        out_specs=(VM, VM, VM, VM),
        scratch_shapes=[
            pltpu.VMEM((4, 64, 2048), BF),
            pltpu.VMEM((256, 2048), BF),
            pltpu.VMEM((2048, 512), BF),
            pltpu.VMEM((2048, 512), BF),
            pltpu.VMEM((2048, 512), BF),
            pltpu.VMEM((2048, 128), BF),
            pltpu.VMEM((2048, 128), BF),
            dma((5,)), dma, dma((2, 2)), dma((2, 2)), dma((2,)), dma((2,)),
        ],
        compiler_params=pltpu.CompilerParams(
            collective_id=0, has_side_effects=True, vmem_limit_bytes=40 * 1024 * 1024
        ),
        name="front",
    )(tokens, norm_gain.reshape(1, -1), wa, wb, wq, wk, wv, query_gain, key_gain)


def middle_kernel(
    kv_in, q_own, q_far, gated, taps, ln_gain, lam, sub_gain,
    attn, conv_out, logs,
    kv, q_in, qpad, m_ref, l_ref, acc, halo, gpad, csum, stat_out, stat_in, ret_out, ret_in, log_out, log_in, log_self,
    lc, ax_s, ax_r, az_s, az_r, bz_s, bz_r, bx_s, bx_r, dd_s, dd_r, ex_s, ex_r, st_s, st_r,
):
    sp, y = lax.axis_index("sp"), lax.axis_index("tp")
    z, x, c = sp // 8, lax.rem(sp // 2, 4), lax.rem(sp, 2)
    sib = 1 - c

    def zm(value):
        return lax.rem(value + 2 * NZ, NZ)

    def xm(value):
        return lax.rem(value + 2 * NX, NX)

    def at(zz, xx, cc):
        return {"sp": zz * 8 + xx * 2 + cc, "tp": y}

    zdev = (at(zm(z + 1), x, c), at(zm(z - 1), x, c))
    xdev = (at(z, xm(x + 1), c), at(z, xm(x - 1), c))
    sdev = at(z, x, sib)
    far_z = NZ - 1 - z
    pdev = at(far_z, x, c)
    nxt = {"sp": lax.rem(sp + 1, 64), "tp": y}
    prv = {"sp": lax.rem(sp + 63, 64), "tp": y}
    ydev = [{"sp": sp, "tp": lax.rem(y + k, NT)} for k in (1, 2, 3)]
    meet = greet([*zdev, *xdev, sdev, pdev, nxt, prv, *ydev])
    sends = []

    def go(copy):
        copy.start()
        sends.append(copy)

    def origin(s, d):
        return zm(z - s) if d == 0 else zm(z + s)

    def signs(s):
        return (0, 1) if 0 < s < 4 else (0,)

    def hop_halves(s, d):
        return (0, 1) if s < 4 else (d,)

    def ax1(d):
        ox = x if d is None else xm(x - 1 + 2 * d)
        return kv.at[c, 0, ox, z]

    def az(s, d, xh, landing):
        return kv.at[c, 0, pl.ds(xh * 2, 2), origin(s if landing else s - 1, d)]

    def bz(s, d, rh, landing):
        return kv.at[c, 1, x, origin(s if landing else s - 1, d), pl.ds(rh * 64, 64)]

    def az_send(s):
        for d in range(2):
            for xh in hop_halves(s, d):
                ref = az(s, d, xh, False)
                go(remote(ref, ref, az_s.at[s - 1, d, xh], az_r.at[s - 1, d, xh], zdev[d]))

    def az_recv(s):
        for d in range(2):
            for xh in hop_halves(s, d):
                ref = az(s, d, xh, True)
                remote(ref, ref, az_s.at[s - 1, d, xh], az_r.at[s - 1, d, xh], zdev[d]).wait_recv()

    def bz_send(s):
        for d in range(2):
            for rh in hop_halves(s, d):
                ref = bz(s, d, rh, False)
                src = kv_in.at[1, pl.ds(rh * 64, 64)] if s == 1 else ref
                go(remote(src, ref, bz_s.at[s - 1, d, rh], bz_r.at[s - 1, d, rh], zdev[d]))

    def bz_recv(s):
        for d in range(2):
            for rh in hop_halves(s, d):
                ref = bz(s, d, rh, True)
                remote(ref, ref, bz_s.at[s - 1, d, rh], bz_r.at[s - 1, d, rh], zdev[d]).wait_recv()

    def bx1_send(s):
        for g in signs(s):
            ref = kv.at[c, 1, x, origin(s, g)]
            for d in range(2):
                go(remote(kv_in.at[1] if s == 0 else ref, ref, bx_s.at[0, s, g, d], bx_r.at[0, s, g, d], xdev[d]))

    def bx1_recv(s):
        for g in signs(s):
            for d in range(2):
                ref = kv.at[c, 1, xm(x - 1 + 2 * d), origin(s, g)]
                remote(ref, ref, bx_s.at[0, s, g, d], bx_r.at[0, s, g, d], xdev[d]).wait_recv()

    def bx2_send(s):
        for g in signs(s):
            for d in range(2):
                ref = kv.at[c, 1, xm(x - 1 + 2 * d), origin(s, g), pl.ds(d * 64, 64)]
                go(remote(ref, ref, bx_s.at[1, s, g, d], bx_r.at[1, s, g, d], xdev[d]))

    def bx2_recv(s):
        for g in signs(s):
            for d in range(2):
                ref = kv.at[c, 1, xm(x + 2), origin(s, g), pl.ds(d * 64, 64)]
                remote(ref, ref, bx_s.at[1, s, g, d], bx_r.at[1, s, g, d], xdev[d]).wait_recv()

    def dd_send(h, s):
        for g in signs(s):
            ref = kv.at[c, h, :, origin(s, g)]
            go(remote(ref, ref, dd_s.at[h, s, g], dd_r.at[h, s, g], sdev))

    def dd_recv(h, s):
        for g in signs(s):
            ref = kv.at[sib, h, :, origin(s, g)]
            remote(ref, ref, dd_s.at[h, s, g], dd_r.at[h, s, g], sdev).wait_recv()

    def tile(which, cc, hh, zt, masked):
        keys = jnp.concatenate([kv[cc, hh, k, zt, :, 0:128] for k in range(NX)], axis=1)
        values = jnp.concatenate([kv[cc, hh, k, zt, :, 128:256] for k in range(NX)], axis=0)
        if masked:
            row = lax.broadcasted_iota(jnp.int32, (256, 128), 0) + (x * 512 + c * 256)
            col = lax.broadcasted_iota(jnp.int32, (256, 128), 1) + (cc * 256 + hh * 128)
        for hm in range(4):
            scores = jnp.dot(qpad[which, hm], keys, preferred_element_type=F32)
            parts = [scores[:, k * 128 : (k + 1) * 128] for k in range(NX)]
            if masked:
                parts = [jnp.where(col + k * 512 <= row, part, -1e30) for k, part in enumerate(parts)]
            top = jnp.maximum(jnp.maximum(parts[0], parts[1]), jnp.maximum(parts[2], parts[3]))
            old = m_ref[which, hm]
            new = jnp.maximum(old, jnp.max(top, axis=1, keepdims=True))
            fade = jnp.exp(old - new)
            parts = [jnp.exp(part - new) for part in parts]
            m_ref[which, hm] = new
            l_ref[which, hm] = l_ref[which, hm] * fade + ((parts[0] + parts[1]) + (parts[2] + parts[3]))
            weights = jnp.concatenate([part.astype(BF) for part in parts], axis=1)
            acc[which, hm] = acc[which, hm] * fade + jnp.dot(weights, values, preferred_element_type=F32)

    def attend(s):
        def step(i, carry):
            which = lax.rem(i, 2)
            hh = lax.rem(i // 2, 2)
            cc = lax.rem(i // 4, 2)
            g = i // 8
            zt = zm(z - s + 2 * s * g)
            zq = jnp.where(which == 0, z, far_z)

            @pl.when(zt < zq)
            def _():
                tile(which, cc, hh, zt, False)

            if s in (0, 1, 3):

                @pl.when(zt == zq)
                def _():
                    tile(which, cc, hh, zt, True)

            return carry

        lax.fori_loop(0, 8 * len(signs(s)), step, 0)

    def stage(e):
        if 1 <= e <= 4:
            bz_recv(e)
            if e < 4:
                bz_send(e + 1)
            bx1_send(e)
        if 0 <= e - 1 <= 4:
            bx1_recv(e - 1)
            bx2_send(e - 1)
        if e == 1:
            for d in range(2):
                ref = ax1(d)
                remote(ref, ref, ax_s.at[0, d], ax_r.at[0, d], xdev[d]).wait_recv()
                ref = kv.at[c, 0, xm(x - 1 + 2 * d), z, pl.ds(d * 64, 64)]
                go(remote(ref, ref, ax_s.at[1, d], ax_r.at[1, d], xdev[d]))
        if e == 2:
            for d in range(2):
                ref = kv.at[c, 0, xm(x + 2), z, pl.ds(d * 64, 64)]
                remote(ref, ref, ax_s.at[1, d], ax_r.at[1, d], xdev[d]).wait_recv()
            az_send(1)
            dd_send(0, 0)
        if 0 <= e - 2 <= 4:
            bx2_recv(e - 2)
            dd_send(1, e - 2)
        if 3 <= e <= 6:
            az_recv(e - 2)
            if e < 6:
                az_send(e - 1)
            dd_send(0, e - 2)
        if e >= 3:
            dd_recv(0, e - 3)
            dd_recv(1, e - 3)
            attend(e - 3)

    own = [pltpu.make_async_copy(kv_in.at[h], kv.at[c, h, x, z], lc.at[h]) for h in range(2)]
    for copy in own:
        copy.start()
    meet()
    for d in range(2):
        go(remote(kv_in.at[0], ax1(None), ax_s.at[0, d], ax_r.at[0, d], xdev[d]))
    bz_send(1)
    bx1_send(0)
    q_copy = remote(q_far, q_in, ex_s.at[0], ex_r.at[0], pdev)
    go(q_copy)
    halo_copy = remote(gated.at[pl.ds(224, 32)], halo, ex_s.at[1], ex_r.at[1], nxt)
    go(halo_copy)
    for copy in own:
        copy.wait()

    m_ref[...] = jnp.full(m_ref.shape, -1e30, F32)
    l_ref[...] = jnp.zeros(l_ref.shape, F32)
    acc[...] = jnp.zeros(acc.shape, F32)
    low = lax.broadcasted_iota(jnp.int32, (256, 128), 1) < 64

    def pad(which, source):
        for k in range(2):
            head = source[:, k * 128 : (k + 1) * 128].astype(F32)
            qpad[which, 2 * k] = jnp.where(low, head, 0.0).astype(BF)
            qpad[which, 2 * k + 1] = jnp.where(low, 0.0, head).astype(BF)

    pad(0, q_own)
    for k in range(4):
        gpad[k, 32:288, :] = gated[:, k * 128 : (k + 1) * 128].astype(F32)
    stage(1)
    halo_copy.wait_recv()
    for k in range(4):
        gpad[k, 0:32, :] = jnp.where(sp > 0, halo[:, k * 128 : (k + 1) * 128].astype(F32), 0.0)
    q_copy.wait_recv()
    pad(1, q_in)

    def conv_step(k, carry):
        one, two = carry
        total = jnp.zeros((256, 128), F32)
        for j in range(KW):
            total = total + taps[k, j : j + 1, :] * gpad[k, j + 2 : j + 258, :]
        csum[k] = total
        return one + total, two + total * total

    nothing = jnp.zeros((256, 128), F32)
    one, two = lax.fori_loop(0, 4, conv_step, (nothing, nothing))
    lane = lax.broadcasted_iota(jnp.int32, (256, 128), 1)
    stat_out[...] = jnp.where(
        lane == 0, jnp.sum(one, axis=1, keepdims=True), jnp.sum(two, axis=1, keepdims=True)
    )
    for k in range(3):
        go(remote(stat_out, stat_in.at[k], st_s.at[k], st_r.at[k], ydev[k]))
    stage(2)
    for k in range(3):
        remote(stat_out, stat_in.at[k], st_s.at[k], st_r.at[k], ydev[k]).wait_recv()
    total = (stat_out[...] + stat_in[0]) + (stat_in[1] + stat_in[2])
    mean = total[:, 0:1] / (NT * 512)
    mean_sq = total[:, 1:2] / (NT * 512)
    scale = lax.rsqrt(mean_sq - mean * mean + 1e-5)
    for k in range(4):
        span = slice(k * 128, (k + 1) * 128)
        conv_out[:, span] = jax.nn.silu((csum[k] - mean) * scale * ln_gain[:, span]).astype(BF)

    for e in range(3, 8):
        stage(e)

    def finish(which, out_ref, log_ref):
        table = jnp.zeros((256, 128), F32)
        for k in range(2):
            outs = []
            for m in range(2):
                total = jnp.sum(l_ref[which, 2 * k + m], axis=1, keepdims=True)
                outs.append(acc[which, 2 * k + m] / total)
                table = jnp.where(lane == 2 * k + m, m_ref[which, 2 * k + m] + jnp.log(total), table)
            row = 2 * which + k
            diff = outs[0] - lam[row : row + 1, :] * outs[1]
            scale = lax.rsqrt(jnp.mean(diff * diff, axis=1, keepdims=True) + 1e-6)
            out_ref[:, k * 128 : (k + 1) * 128] = (diff * scale * sub_gain[...]).astype(BF)
        log_ref[...] = table.T[0:8, :]

    finish(1, ret_out, log_out)
    back = [
        remote(ret_out, ret_in, ex_s.at[2], ex_r.at[2], pdev),
        remote(log_out, log_in, ex_s.at[3], ex_r.at[3], pdev),
    ]
    for copy in back:
        go(copy)
    finish(0, attn.at[:, pl.ds(0, 256)], log_self)
    for k in range(2):
        for m in range(2):
            logs[m, k : k + 1, :] = log_self[2 * k + m : 2 * k + m + 1, :]
    for copy in back:
        copy.wait_recv()
    attn[:, 256:512] = ret_in[...]
    for k in range(2):
        for m in range(2):
            logs[m, 2 + k : 3 + k, :] = log_in[2 * k + m : 2 * k + m + 1, :]
    for copy in sends:
        copy.wait_send()


def middle(kv, q_own, q_far, gated, taps, ln_gain, lam_head, sub_gain):
    dma = pltpu.SemaphoreType.DMA
    taps = taps.reshape(KW, 4, 128).transpose(1, 0, 2)
    lam = jnp.broadcast_to(lam_head[:, None], (4, 128))
    return pl.pallas_call(
        middle_kernel,
        out_shape=(
            jax.ShapeDtypeStruct((256, 512), BF),
            jax.ShapeDtypeStruct((256, 512), BF),
            jax.ShapeDtypeStruct((2, 4, 256), F32),
        ),
        in_specs=[VM] * 8,
        out_specs=(VM, VM, VM),
        scratch_shapes=[
            pltpu.VMEM((2, 2, NX, NZ, 128, 256), BF),
            pltpu.VMEM((256, 256), BF),
            pltpu.VMEM((2, 4, 256, 128), BF),
            pltpu.VMEM((2, 4, 256, 128), F32),
            pltpu.VMEM((2, 4, 256, 128), F32),
            pltpu.VMEM((2, 4, 256, 128), F32),
            pltpu.VMEM((32, 512), BF),
            pltpu.VMEM((4, 288, 128), F32),
            pltpu.VMEM((4, 256, 128), F32),
            pltpu.VMEM((256, 128), F32),
            pltpu.VMEM((3, 256, 128), F32),
            pltpu.VMEM((256, 256), BF),
            pltpu.VMEM((256, 256), BF),
            pltpu.VMEM((8, 256), F32),
            pltpu.VMEM((8, 256), F32),
            pltpu.VMEM((8, 256), F32),
            dma((2,)),
            dma((2, 2)), dma((2, 2)),
            dma((4, 2, 2)), dma((4, 2, 2)),
            dma((4, 2, 2)), dma((4, 2, 2)),
            dma((2, 5, 2, 2)), dma((2, 5, 2, 2)),
            dma((2, 5, 2)), dma((2, 5, 2)),
            dma((4,)), dma((4,)),
            dma((3,)), dma((3,)),
        ],
        compiler_params=pltpu.CompilerParams(
            collective_id=1, has_side_effects=True, vmem_limit_bytes=44 * 1024 * 1024
        ),
        name="middle",
    )(kv, q_own, q_far, gated, taps, ln_gain.reshape(1, -1), lam, sub_gain.reshape(1, -1))


def back_kernel(conv, attn, w_conv, w_attn, mixed, part, far, near, total, r1, r2, s1, q1, s2, q2):
    y = lax.axis_index("tp")
    targets = ({"tp": lax.rem(y + 1, NT)}, {"tp": lax.rem(y + 3, NT)})
    meet = greet(targets)
    own = lax.rem(y + 4, NT)
    blocks = (lax.rem(y + 1, NT), lax.rem(y + 3, NT))
    opposite = lax.rem(y + 2, NT)
    sends = []

    def go(copy):
        copy.start()
        sends.append(copy)

    def rows(block):
        return pl.ds(pl.multiple_of(block * 64, 64), 64)

    for n in range(4):
        span = pl.ds(n * 512, 512)
        part[:, span] = jnp.dot(conv[...], w_conv[:, span], preferred_element_type=F32) + jnp.dot(
            attn[...], w_attn[:, span], preferred_element_type=F32
        )
        if n % 2 == 1:
            d = n // 2
            wide = pl.ds(d * 1024, 1024)
            far[d] = part[rows(opposite), wide].astype(BF)
            near[d] = part[rows(blocks[1 - d]), wide].astype(BF)
            if d == 0:
                meet()
            go(remote(far.at[d], r1.at[d], s1.at[d], q1.at[d], targets[d]))
            go(remote(near.at[d], r2.at[1 - d, d], s2.at[1 - d, d], q2.at[1 - d, d], targets[1 - d]))
    for d in range(2):
        remote(far.at[d], r1.at[d], s1.at[d], q1.at[d], targets[d]).wait_recv()
        wide = pl.ds(d * 1024, 1024)
        total[d] = (part[rows(blocks[d]), wide] + r1[d].astype(F32)).astype(BF)
        go(remote(total.at[d], r2.at[d, d], s2.at[d, d], q2.at[d, d], targets[d]))
    for d in (1, 0):
        for k in (1 - d, d):
            remote(total.at[d], r2.at[k, d], s2.at[k, d], q2.at[k, d], targets[k]).wait_recv()
        wide = pl.ds(d * 1024, 1024)
        mixed[:, wide] = (part[rows(own), wide] + (r2[0, d].astype(F32) + r2[1, d].astype(F32))).astype(BF)
    for copy in sends:
        copy.wait_send()


def back(conv, attn, w_conv, w_attn):
    dma = pltpu.SemaphoreType.DMA
    return pl.pallas_call(
        back_kernel,
        out_shape=jax.ShapeDtypeStruct((64, 2048), BF),
        in_specs=[VM] * 4,
        out_specs=VM,
        scratch_shapes=[
            pltpu.VMEM((256, 2048), F32),
            pltpu.VMEM((2, 64, 1024), BF),
            pltpu.VMEM((2, 64, 1024), BF),
            pltpu.VMEM((2, 64, 1024), BF),
            pltpu.VMEM((2, 64, 1024), BF),
            pltpu.VMEM((2, 2, 64, 1024), BF),
            dma((2,)), dma((2,)), dma((2, 2)), dma((2, 2)),
        ],
        compiler_params=pltpu.CompilerParams(
            collective_id=2, has_side_effects=True, vmem_limit_bytes=24 * 1024 * 1024
        ),
        name="back",
    )(conv, attn, w_conv, w_attn)


def on_device(
    tokens, norm_gain, w_glu_a, w_glu_b, conv_taps, ln_gain, w_query, w_key, w_value,
    query_gain, key_gain, lam_head, sub_gain, w_out_conv, w_out_attn,
):
    gated, q_own, q_far, kv = front(
        tokens, norm_gain, w_glu_a, w_glu_b, w_query, w_key, w_value, query_gain, key_gain
    )
    attn, conv_out, logs = middle(kv, q_own, q_far, gated, conv_taps, ln_gain, lam_head, sub_gain)
    return back(conv_out, attn, w_out_conv, w_out_attn), logs


def solution(mesh):
    return jax.shard_map(
        on_device,
        mesh=mesh,
        in_specs=(
            P(("sp", "tp"), None), P(), P(None, "tp"), P(None, "tp"), P(None, "tp"), P("tp"),
            P(None, "tp"), P(None, "tp"), P(None, "tp"), P("tp", None), P("tp", None), P("tp"),
            P(), P("tp", None), P("tp", None),
        ),
        out_specs=(P(("sp", "tp"), None), P(None, "tp", "sp")),
        check_vma=False,
    )
```

time: 387 us -> 132 us (0.34); the launches traced: 381 us -> 131 us
  Pallas kernels: 0 us -> 118 us
  waiting for transfers between devices: 104 us -> 0 us
  other arithmetic: 86.7 us -> 0 us
  matrix products: 84.3 us -> 0 us
  local copies, waits for them, and re-layouts: 69.5 us -> 12.7 us
  between operations: 14.3 us -> 0.72 us
  loops' own time: 11.6 us -> 0 us
  starting transfers between devices: 9.71 us -> 0 us
    pallas_call x0 -> x3, Pallas kernels: none -> 118 us  [the longest x1 92.4 us: middle(): pl.pallas_call(middle_kernel, out_shape=(jax.ShapeDtypeStruct((256, 512),...]
    dot_general x39 -> x0, matrix products: 84.3 us -> none  [the longest x16 46.7 us: attend_rows(): jnp.einsum('kgmtr,rkv->kgmtv', weights.astype(jnp.bfloat16), value_grid,...]
    all_gather x2 -> x0, waiting for transfers between devices: 81.1 us -> none  [the longest x1 52.1 us: sent_together(): filled = lax.all_gather(both, axis, axis=dim, tiled=True)]
    another operation x16 -> x0, other arithmetic: 37.4 us -> none
    dynamic_slice x48 -> x0, local copies, waits for them, and re-layouts: 27.6 us -> none  [attend_span(): lax.scan(one_step, totals, (key_blocks, value_blocks, jnp.arange(step_cou...]
    add x48 -> x0, other arithmetic: 20.8 us -> none  [the longest x16 20.7 us: attend_rows(): new_sum = run_sum * rescale + jnp.sum(weights, axis=-1)]
    all_to_all x2 -> x0, waiting for transfers between devices: 19.3 us -> none  [the longest x1 14.2 us: sum_at_owner(): lax.all_to_all(cut_along(value, dim, count), axis, 0, 0, tiled=True)]
    while x80 -> x0, local copies, waits for them, and re-layouts: 15.5 us -> none
  transfers between devices with their start and end apart: 5 -> 0, of which waited for: 5 -> 0; matrix products, arithmetic and copies ran while one was open for 5% -> 0% of each run, Pallas kernels for 0% -> 0%
where the time goes in v1:
time: 132 us; the launch traced here: 131 us
  Pallas kernels  118 us (89%)
  local copies, waits for them, and re-layouts  12.7 us (10%)
    pallas_call x1, Pallas kernels, middle(): pl.pallas_call(middle_kernel, out_shape=(jax.ShapeDtypeStruct((256, 512),...  92.4 us
    pallas_call x1, Pallas kernels, front(): pl.pallas_call(front_kernel, out_shape=(jax.ShapeDtypeStruct((256, 512),...  15.2 us
    unnamed x28, local copies, waits for them, and re-layouts  11.1 us
    pallas_call x1, Pallas kernels, back(): pl.pallas_call(back_kernel, out_shape=jax.ShapeDtypeStruct((64, 2048), BF...  10.2 us

profile of v1, /device:TPU:64, one launch (start us, length us, event | category | flops | bytes accessed | tf_op | source)
XLA Modules:
  0.0 131.3 jit_solution(17575459675197473183)
XLA Ops:
  0.6 0.7 broadcast_in_dim.2.lam
  1.4 0.9 reshape.18
  2.2 0.0 copy-start
  2.2 1.6 %copy-done = bf16[2048,512]{1,0:T(8,128)(2,1)S(1)} copy-done((bf16[2048,512]{1,0:T(8,128)(2,1)S(1)}, bf16[2048,512]{1,0:T(8,128)(2,1)}, u32[]{:S(2)}) %copy-start) | copy-done | bytes 2097176
  3.8 0.0 copy-start.1
  3.8 1.6 %copy-done.1 = bf16[2048,512]{1,0:T(8,128)(2,1)S(1)} copy-done((bf16[2048,512]{1,0:T(8,128)(2,1)S(1)}, bf16[2048,512]{1,0:T(8,128)(2,1)}, u32[]{:S(2)}) %copy-start.1) | copy-done | bytes 2097176
  5.4 0.0 copy-start.2
  5.4 1.6 %copy-done.2 = bf16[2048,512]{1,0:T(8,128)(2,1)S(1)} copy-done((bf16[2048,512]{1,0:T(8,128)(2,1)S(1)}, bf16[2048,512]{1,0:T(8,128)(2,1)}, u32[]{:S(2)}) %copy-start.2) | copy-done | bytes 2097176
  7.0 0.0 copy-start.5
  7.0 1.0 copy-done.5
  8.1 0.0 copy-start.6
  8.1 1.0 copy-done.6
  9.1 0.0 copy-start.7
  9.1 0.9 copy-done.7
  10.0 0.0 copy-start.8
  10.0 0.7 copy-done.8
  10.7 0.0 copy-start.9
  10.7 0.7 copy-done.9
  11.4 0.0 copy-start.11
  11.4 0.7 copy-done.11
  12.1 0.0 copy-start.10
  12.1 0.0 copy-start.12
  12.1 0.0 copy-start.3
  12.1 0.0 copy-start.4
  12.1 15.2 %front.1 = (bf16[256,512]{1,0:T(8,128)(2,1)S(1)}, bf16[256,256]{1,0:T(8,128)(2,1)S(1)}, bf16[256,256]{1,0:T(8,128)(2,1)S(1)}, bf16[2,128,256]{2,1,0:T(8,128)(2,1)S(1)}) custom-call(bf16[64,2048]{1,0:T(8,128)(2,1)S(1)} %copy-done.7, f32[1,2048]{1,0:T(1,128)S(1)} %bitcast.7, bf16[2048,512]{1,0:T(8,128)(2,1)S(1)} %copy-done, bf16[2048,512]{1,0:T(8,128)(2,1)S(1)} %copy-done.1, ...), custom_call_target="tpu_custom_call" | custom-call | tf_op jit(solution)/shard_map/front/pallas_call | solution.py:118
  27.3 0.0 copy-done.10
  27.3 0.0 copy-done.12
  27.3 92.4 %middle.1 = (bf16[256,512]{1,0:T(8,128)(2,1)S(1)}, bf16[256,512]{1,0:T(8,128)(2,1)S(1)}, f32[2,4,256]{2,1,0:T(4,128)S(1)}) custom-call(bf16[2,128,256]{2,1,0:T(8,128)(2,1)S(1)} %get-tuple-element.9.kv_in, bf16[256,256]{1,0:T(8,128)(2,1)S(1)} %get-tuple-element.10.q_own, bf16[256,256]{1,0:T(8,128)(2,1)S(1)} %get-tuple-element.11.q_far, ...), custom_call_target="tpu_custom_call" | custom-call | tf_op jit(solution)/shard_map/middle/pallas_call | solution.py:440
  119.7 0.0 copy-done.3
  119.7 0.0 copy-done.4
  119.7 10.2 %back.1 = bf16[64,2048]{1,0:T(8,128)(2,1)S(1)} custom-call(bf16[256,512]{1,0:T(8,128)(2,1)S(1)} %get-tuple-element.13.conv, bf16[256,512]{1,0:T(8,128)(2,1)S(1)} %get-tuple-element.14.attn, bf16[512,2048]{1,0:T(8,128)(2,1)S(1)} %copy-done.3, bf16[512,2048]{1,0:T(8,128)(2,1)S(1)} %copy-done.4), custom_call_target="tpu_custom_call" | custom-call | tf_op jit(solution)/shard_map/back/pallas_call | solution.py:528
  130.0 0.7 copy.22
  130.7 0.6 copy.23
  (1 shorter events, 0.0 us)
Async XLA Ops:
  2.2 1.6 %copy-start = (bf16[2048,512]{1,0:T(8,128)(2,1)S(1)}, bf16[2048,512]{1,0:T(8,128)(2,1)}, u32[]{:S(2)}) copy-start(bf16[2048,512]{1,0:T(8,128)(2,1)} %wa_h.1) | copy-start | bytes 6291460
  3.8 1.6 %copy-start.1 = (bf16[2048,512]{1,0:T(8,128)(2,1)S(1)}, bf16[2048,512]{1,0:T(8,128)(2,1)}, u32[]{:S(2)}) copy-start(bf16[2048,512]{1,0:T(8,128)(2,1)} %wb_h.1) | copy-start | bytes 6291460
  5.4 1.6 %copy-start.2 = (bf16[2048,512]{1,0:T(8,128)(2,1)S(1)}, bf16[2048,512]{1,0:T(8,128)(2,1)}, u32[]{:S(2)}) copy-start(bf16[2048,512]{1,0:T(8,128)(2,1)} %wq_h.1) | copy-start | bytes 6291460
  7.0 1.0 copy-start.5
  8.1 1.0 copy-start.6
  9.1 0.9 copy-start.7
  10.0 0.7 copy-start.8
  10.7 0.7 copy-start.9
  11.4 0.7 copy-start.11
  12.1 15.2 %copy-start.10 = (f32[512]{0:T(512)S(1)}, f32[512]{0:T(512)}, u32[]{:S(2)}) copy-start(f32[512]{0:T(512)} %param.20) | copy-start | bytes 6148
  12.1 15.2 %copy-start.12 = (f32[128]{0:T(128)S(1)}, f32[128]{0:T(128)}, u32[]{:S(2)}) copy-start(f32[128]{0:T(128)} %param.27) | copy-start | bytes 1540
  12.1 107.6 %copy-start.3 = (bf16[512,2048]{1,0:T(8,128)(2,1)S(1)}, bf16[512,2048]{1,0:T(8,128)(2,1)}, u32[]{:S(2)}) copy-start(bf16[512,2048]{1,0:T(8,128)(2,1)} %w_conv.1) | copy-start | bytes 6291460
  12.1 107.6 %copy-start.4 = (bf16[512,2048]{1,0:T(8,128)(2,1)S(1)}, bf16[512,2048]{1,0:T(8,128)(2,1)}, u32[]{:S(2)}) copy-start(bf16[512,2048]{1,0:T(8,128)(2,1)} %w_attn.1) | copy-start | bytes 6291460

commit v2 on v1

v2 whole, which is shorter than its diff:
```python
import functools

import jax
import jax.numpy as jnp
from jax import lax
from jax.experimental import pallas as pl
from jax.experimental.pallas import tpu as pltpu
from jax.sharding import PartitionSpec as P

KW = 31
MESH = pl.DeviceIdType.MESH
NZ, NX, NT = 8, 4, 4
BF, F32 = jnp.bfloat16, jnp.float32
VM = pl.BlockSpec(memory_space=pltpu.VMEM)


def remote(src, dst, send, recv, device):
    return pltpu.make_async_remote_copy(
        src_ref=src, dst_ref=dst, send_sem=send, recv_sem=recv, device_id=device, device_id_type=MESH
    )


def greet(devices):
    barrier = pltpu.get_barrier_semaphore()
    for device in devices:
        pl.semaphore_signal(barrier, inc=1, device_id=device, device_id_type=MESH)
    return lambda: pl.semaphore_wait(barrier, len(devices))


def half_norm(value, gain):
    low = lax.broadcasted_iota(jnp.int32, value.shape, 1) < 64
    squares = value * value
    first = jnp.sum(jnp.where(low, squares, 0.0), axis=1, keepdims=True)
    second = jnp.sum(jnp.where(low, 0.0, squares), axis=1, keepdims=True)
    scale = jnp.where(low, lax.rsqrt(first / 64 + 1e-6), lax.rsqrt(second / 64 + 1e-6))
    return (value * scale * gain).astype(BF)


HBM = pl.BlockSpec(memory_space=pltpu.MemorySpace.HBM)
SM = pl.BlockSpec(memory_space=pltpu.SMEM)


def layer_kernel(
    tok, gain, wa_h, wb_h, wq_h, wk_h, wv_h, qg, kg, taps, ln_gain, lam, sub_gain, wc_h, wo_h,
    mixed, logs,
    rows, normed, wa, wb, wq, wk, wv, wc, wo, gated, kv_in, q_own, q_far,
    kv, q_in, qpad, m_ref, l_ref, acc, halo, gpad, csum, stat_out, stat_in,
    attn, conv_out, ret_out, ret_in, log_out, log_in, log_self,
    part, far, near, total_out, r1, r2,
    w_sem, own_sem, y1s, y1r, y2s, y2r,
    lc, ax_s, ax_r, az_s, az_r, bz_s, bz_r, bx_s, bx_r, dd_s, dd_r, ex_s, ex_r, st_s, st_r,
    o1s, o1r, o2s, o2r,
):
    sp, y = lax.axis_index("sp"), lax.axis_index("tp")
    z, x, c = sp // 8, lax.rem(sp // 2, 4), lax.rem(sp, 2)
    sib = 1 - c

    def zm(value):
        return lax.rem(value + 2 * NZ, NZ)

    def xm(value):
        return lax.rem(value + 2 * NX, NX)

    def at(zz, xx, cc):
        return {"sp": zz * 8 + xx * 2 + cc, "tp": y}

    zdev = (at(zm(z + 1), x, c), at(zm(z - 1), x, c))
    xdev = (at(z, xm(x + 1), c), at(z, xm(x - 1), c))
    sdev = at(z, x, sib)
    far_z = NZ - 1 - z
    pdev = at(far_z, x, c)
    nxt = {"sp": lax.rem(sp + 1, 64), "tp": y}
    prv = {"sp": lax.rem(sp + 63, 64), "tp": y}
    ydev = [{"sp": sp, "tp": lax.rem(y + k, NT)} for k in (1, 2, 3)]
    up, down = ydev[0], ydev[2]
    meet = greet([*zdev, *xdev, sdev, pdev, nxt, prv, *ydev])
    sends = []

    def go(copy):
        copy.start()
        sends.append(copy)

    def origin(s, d):
        return zm(z - s) if d == 0 else zm(z + s)

    def signs(s):
        return (0, 1) if 0 < s < 4 else (0,)

    def hop_halves(s, d):
        return (0, 1) if s < 4 else (d,)

    def ax1(d):
        ox = x if d is None else xm(x - 1 + 2 * d)
        return kv.at[c, 0, ox, z]

    def az(s, d, xh, landing):
        return kv.at[c, 0, pl.ds(xh * 2, 2), origin(s if landing else s - 1, d)]

    def bz(s, d, rh, landing):
        return kv.at[c, 1, x, origin(s if landing else s - 1, d), pl.ds(rh * 64, 64)]

    def az_send(s, xh):
        for d in range(2):
            if xh in hop_halves(s, d):
                ref = az(s, d, xh, False)
                go(remote(ref, ref, az_s.at[s - 1, d, xh], az_r.at[s - 1, d, xh], zdev[d]))

    def az_recv(s, xh):
        for d in range(2):
            if xh in hop_halves(s, d):
                ref = az(s, d, xh, True)
                remote(ref, ref, az_s.at[s - 1, d, xh], az_r.at[s - 1, d, xh], zdev[d]).wait_recv()

    def bz_send(s):
        for d in range(2):
            for rh in hop_halves(s, d):
                ref = bz(s, d, rh, False)
                src = kv_in.at[1, pl.ds(rh * 64, 64)] if s == 1 else ref
                go(remote(src, ref, bz_s.at[s - 1, d, rh], bz_r.at[s - 1, d, rh], zdev[d]))

    def bz_recv(s):
        for d in range(2):
            for rh in hop_halves(s, d):
                ref = bz(s, d, rh, True)
                remote(ref, ref, bz_s.at[s - 1, d, rh], bz_r.at[s - 1, d, rh], zdev[d]).wait_recv()

    def bx1_send(s):
        for g in signs(s):
            ref = kv.at[c, 1, x, origin(s, g)]
            for d in range(2):
                go(remote(kv_in.at[1] if s == 0 else ref, ref, bx_s.at[0, s, g, d], bx_r.at[0, s, g, d], xdev[d]))

    def bx1_recv(s):
        for g in signs(s):
            for d in range(2):
                ref = kv.at[c, 1, xm(x - 1 + 2 * d), origin(s, g)]
                remote(ref, ref, bx_s.at[0, s, g, d], bx_r.at[0, s, g, d], xdev[d]).wait_recv()

    def bx2_send(s):
        for g in signs(s):
            for d in range(2):
                ref = kv.at[c, 1, xm(x - 1 + 2 * d), origin(s, g), pl.ds(d * 64, 64)]
                go(remote(ref, ref, bx_s.at[1, s, g, d], bx_r.at[1, s, g, d], xdev[d]))

    def bx2_recv(s):
        for g in signs(s):
            for d in range(2):
                ref = kv.at[c, 1, xm(x + 2), origin(s, g), pl.ds(d * 64, 64)]
                remote(ref, ref, bx_s.at[1, s, g, d], bx_r.at[1, s, g, d], xdev[d]).wait_recv()

    def dd_send(h, s):
        for g in signs(s):
            ref = kv.at[c, h, :, origin(s, g)]
            go(remote(ref, ref, dd_s.at[h, s, g], dd_r.at[h, s, g], sdev))

    def dd_recv(h, s):
        for g in signs(s):
            ref = kv.at[sib, h, :, origin(s, g)]
            remote(ref, ref, dd_s.at[h, s, g], dd_r.at[h, s, g], sdev).wait_recv()

    def tile(which, cc, zt, masked):
        pieces = [(h, k) for h in range(2) for k in range(NX)]
        keys = jnp.concatenate([kv[cc, h, k, zt, :, 0:128] for h, k in pieces], axis=1)
        values = jnp.concatenate([kv[cc, h, k, zt, :, 128:256] for h, k in pieces], axis=0)
        if masked:
            row = lax.broadcasted_iota(jnp.int32, (256, 128), 0) + (x * 512 + c * 256)
            col = lax.broadcasted_iota(jnp.int32, (256, 128), 1) + cc * 256
        scores = jnp.dot(qpad[which].reshape(1024, 128), keys, preferred_element_type=F32)
        weights, fades = [], []
        for hm in range(4):
            parts = [scores[hm * 256 : (hm + 1) * 256, k * 128 : (k + 1) * 128] for k in range(8)]
            if masked:
                parts = [
                    jnp.where(col + (h * 128 + k * 512) <= row, item, -1e30)
                    for item, (h, k) in zip(parts, pieces)
                ]
            old = m_ref[which, hm]
            new = jnp.maximum(old, jnp.max(functools.reduce(jnp.maximum, parts), axis=1, keepdims=True))
            fade = jnp.exp(old - new)
            parts = [jnp.exp(item - new) for item in parts]
            m_ref[which, hm] = new
            l_ref[which, hm] = l_ref[which, hm] * fade + functools.reduce(jnp.add, parts)
            weights.append(jnp.concatenate([item.astype(BF) for item in parts], axis=1))
            fades.append(fade)
        outs = jnp.dot(jnp.concatenate(weights, axis=0), values, preferred_element_type=F32)
        for hm in range(4):
            acc[which, hm] = acc[which, hm] * fades[hm] + outs[hm * 256 : (hm + 1) * 256]

    def attend(s, g, cores):
        zt = zm(z - s + 2 * s * g)

        def step(i, carry):
            which = lax.rem(i, 2)
            cc = lax.rem(c + i // 2, 2)
            zq = jnp.where(which == 0, z, far_z)

            @pl.when(zt < zq)
            def _():
                tile(which, cc, zt, False)

            if s in (0, 1, 3):

                @pl.when(zt == zq)
                def _():
                    tile(which, cc, zt, True)

            return carry

        lax.fori_loop(2 * cores[0], 2 * cores[1], step, 0)

    def stage(e):
        if 1 <= e <= 4:
            bz_recv(e)
            if e < 4:
                bz_send(e + 1)
            bx1_send(e)
        if 0 <= e - 1 <= 4:
            bx1_recv(e - 1)
            bx2_send(e - 1)
        if e == 1:
            for d in range(2):
                ref = ax1(d)
                remote(ref, ref, ax_s.at[0, d], ax_r.at[0, d], xdev[d]).wait_recv()
                ref = kv.at[c, 0, xm(x - 1 + 2 * d), z, pl.ds(d * 64, 64)]
                go(remote(ref, ref, ax_s.at[1, d], ax_r.at[1, d], xdev[d]))
        if e == 2:
            for d in range(2):
                ref = kv.at[c, 0, xm(x + 2), z, pl.ds(d * 64, 64)]
                remote(ref, ref, ax_s.at[1, d], ax_r.at[1, d], xdev[d]).wait_recv()
            az_send(1, 0)
            az_send(1, 1)
            dd_send(0, 0)
        if 0 <= e - 2 <= 4:
            bx2_recv(e - 2)
            dd_send(1, e - 2)
        if e == 3:
            attend(0, 0, (0, 1))
        for xh in range(2):
            if 3 <= e <= 6:
                az_recv(e - 2, xh)
                if e < 6:
                    az_send(e - 1, xh)
            if e > 3 and xh == 0:
                dd_recv(0, e - 3)
                dd_recv(1, e - 3)
                attend(e - 3, 0, (0, 2))
        if 3 <= e <= 6:
            dd_send(0, e - 2)
        if e == 3:
            dd_recv(0, 0)
            dd_recv(1, 0)
            attend(0, 0, (1, 2))
        elif 3 < e < 7:
            attend(e - 3, 1, (0, 2))

    pairs = ((wk_h, wk), (wv_h, wv), (wq_h, wq), (wa_h, wa), (wb_h, wb), (wc_h, wc), (wo_h, wo))
    loads = [pltpu.make_async_copy(src, dst, w_sem.at[i]) for i, (src, dst) in enumerate(pairs)]
    own_rows = pltpu.make_async_copy(tok, rows.at[y], own_sem)
    own_rows.start()
    meet()

    def piece(slot, half):
        return rows.at[slot, pl.ds(half * 32, 32)]

    ypair = ((up, lax.rem(y + 3, NT)), (down, lax.rem(y + 1, NT)))
    for order in range(2):
        for d in range(2):
            half = order if d == 0 else 1 - order
            go(remote(tok.at[pl.ds(half * 32, 32)], piece(y, half), y1s.at[d, half], y1r.at[d, half], ypair[d][0]))
    for load in loads:
        load.start()
    own_rows.wait()

    def norm_slot(slot):
        value = rows[slot].astype(F32)
        scale = lax.rsqrt(jnp.mean(value * value, axis=1, keepdims=True) + 1e-6)
        normed[pl.ds(pl.multiple_of(slot * 64, 64), 64), :] = (value * scale * gain[...]).astype(BF)

    norm_slot(y)
    m_ref[...] = jnp.full(m_ref.shape, -1e30, F32)
    l_ref[...] = jnp.zeros(l_ref.shape, F32)
    acc[...] = jnp.zeros(acc.shape, F32)
    for d in range(2):
        target, source = ypair[d]
        ref = piece(source, d)
        remote(ref, ref, y1s.at[d, d], y1r.at[d, d], target).wait_recv()
        go(remote(ref, ref, y2s.at[d], y2r.at[d], target))
    for d in range(2):
        target, source = ypair[d]
        ref = piece(source, 1 - d)
        remote(ref, ref, y1s.at[d, 1 - d], y1r.at[d, 1 - d], target).wait_recv()
        norm_slot(source)
    opposite = lax.rem(y + 2, NT)
    for d in range(2):
        ref = piece(opposite, d)
        remote(ref, ref, y2s.at[d], y2r.at[d], ypair[d][0]).wait_recv()
    norm_slot(opposite)

    def dot(weight):
        return jnp.dot(normed[...], weight, preferred_element_type=F32)

    for load in loads[:3]:
        load.wait()
    key_value = dot(jnp.concatenate([wk[...], wv[...]], axis=1))
    keys_all = half_norm(key_value[:, :128], kg[...])
    for h in range(2):
        kv_in[h, :, 0:128] = keys_all[h * 128 : (h + 1) * 128].T
        kv_in[h, :, 128:256] = key_value[h * 128 : (h + 1) * 128, 128:].astype(BF)

    def project_q(n, target):
        queries = dot(wq[:, n * 256 : (n + 1) * 256])
        for k in range(2):
            one = half_norm(queries[:, k * 128 : (k + 1) * 128], qg[2 * n + k : 2 * n + k + 1, :])
            target[:, k * 128 : (k + 1) * 128] = one * jnp.asarray(0.125, BF)

    project_q(1, q_far)
    own = [pltpu.make_async_copy(kv_in.at[h], kv.at[c, h, x, z], lc.at[h]) for h in range(2)]
    for copy in own:
        copy.start()
    for d in range(2):
        go(remote(kv_in.at[0], ax1(None), ax_s.at[0, d], ax_r.at[0, d], xdev[d]))
    bz_send(1)
    bx1_send(0)
    for load in loads[3:5]:
        load.wait()
    for n in range(2):
        span = slice(n * 256, (n + 1) * 256)
        gated[:, span] = (dot(wa[:, span]) * jax.nn.sigmoid(dot(wb[:, span]))).astype(BF)
    q_copy = remote(q_far, q_in, ex_s.at[0], ex_r.at[0], pdev)
    go(q_copy)
    project_q(0, q_own)
    halo_copy = remote(gated.at[pl.ds(224, 32)], halo, ex_s.at[1], ex_r.at[1], nxt)
    go(halo_copy)
    for copy in own:
        copy.wait()
    stage(1)
    low = lax.broadcasted_iota(jnp.int32, (256, 128), 1) < 64

    def pad(which, source):
        for k in range(2):
            head = source[:, k * 128 : (k + 1) * 128].astype(F32)
            qpad[which, 2 * k] = jnp.where(low, head, 0.0).astype(BF)
            qpad[which, 2 * k + 1] = jnp.where(low, 0.0, head).astype(BF)

    pad(0, q_own)
    for k in range(4):
        gpad[k, 32:288, :] = gated[:, k * 128 : (k + 1) * 128].astype(F32)
    halo_copy.wait_recv()
    for k in range(4):
        gpad[k, 0:32, :] = jnp.where(sp > 0, halo[:, k * 128 : (k + 1) * 128].astype(F32), 0.0)

    def conv_step(k, carry):
        one, two = carry
        total = jnp.zeros((256, 128), F32)
        lanes = pl.ds(pl.multiple_of(k * 128, 128), 128)
        for j in range(KW):
            total = total + taps[j : j + 1, lanes] * gpad[k, j + 2 : j + 258, :]
        csum[k] = total
        return one + total, two + total * total

    nothing = jnp.zeros((256, 128), F32)
    one, two = lax.fori_loop(0, 2, conv_step, (nothing, nothing))
    stage(2)
    one, two = lax.fori_loop(2, 4, conv_step, (one, two))
    lane = lax.broadcasted_iota(jnp.int32, (256, 128), 1)
    stat_out[...] = jnp.where(
        lane == 0, jnp.sum(one, axis=1, keepdims=True), jnp.sum(two, axis=1, keepdims=True)
    )
    q_copy.wait_recv()
    pad(1, q_in)
    for k in range(3):
        go(remote(stat_out, stat_in.at[k], st_s.at[k], st_r.at[k], ydev[k]))
    stage(3)
    for k in range(3):
        remote(stat_out, stat_in.at[k], st_s.at[k], st_r.at[k], ydev[k]).wait_recv()
    total = (stat_out[...] + stat_in[0]) + (stat_in[1] + stat_in[2])
    mean = total[:, 0:1] / (NT * 512)
    mean_sq = total[:, 1:2] / (NT * 512)
    scale = lax.rsqrt(mean_sq - mean * mean + 1e-5)
    for k in range(4):
        span = slice(k * 128, (k + 1) * 128)
        conv_out[:, span] = jax.nn.silu((csum[k] - mean) * scale * ln_gain[:, span]).astype(BF)
    for load in loads[5:]:
        load.wait()
    for n in range(4):
        span = pl.ds(n * 512, 512)
        part[:, span] = jnp.dot(conv_out[...], wc[:, span], preferred_element_type=F32)

    for e in range(4, 8):
        stage(e)

    def finish(which, out_ref, log_ref):
        table = jnp.zeros((256, 128), F32)
        for k in range(2):
            outs = []
            for m in range(2):
                total = jnp.sum(l_ref[which, 2 * k + m], axis=1, keepdims=True)
                outs.append(acc[which, 2 * k + m] / total)
                table = jnp.where(lane == 2 * k + m, m_ref[which, 2 * k + m] + jnp.log(total), table)
            row = 2 * which + k
            diff = outs[0] - lam[row] * outs[1]
            scale = lax.rsqrt(jnp.mean(diff * diff, axis=1, keepdims=True) + 1e-6)
            out_ref[:, k * 128 : (k + 1) * 128] = (diff * scale * sub_gain[...]).astype(BF)
        log_ref[...] = table.T[0:8, :]

    finish(1, ret_out, log_out)
    back = [
        remote(ret_out, ret_in, ex_s.at[2], ex_r.at[2], pdev),
        remote(log_out, log_in, ex_s.at[3], ex_r.at[3], pdev),
    ]
    for copy in back:
        go(copy)
    finish(0, attn, log_self)
    for n in range(4):
        span = pl.ds(n * 512, 512)
        part[:, span] += jnp.dot(attn[...], wo[0:256, span], preferred_element_type=F32)
    for copy in back:
        copy.wait_recv()
    for which, table in ((0, log_self), (1, log_in)):
        for k in range(2):
            for m in range(2):
                logs[m, 2 * which + k : 2 * which + k + 1, :] = table[2 * k + m : 2 * k + m + 1, :]

    targets = (up, down)
    blocks = (lax.rem(y + 1, NT), lax.rem(y + 3, NT))

    def block_rows(block):
        return pl.ds(pl.multiple_of(block * 64, 64), 64)

    for n in range(4):
        span = pl.ds(n * 512, 512)
        part[:, span] += jnp.dot(ret_in[...], wo[256:512, span], preferred_element_type=F32)
        if n % 2 == 1:
            d = n // 2
            wide = pl.ds(d * 1024, 1024)
            far[d] = part[block_rows(opposite), wide].astype(BF)
            near[d] = part[block_rows(blocks[1 - d]), wide].astype(BF)
            go(remote(far.at[d], r1.at[d], o1s.at[d], o1r.at[d], targets[d]))
            go(remote(near.at[d], r2.at[1 - d, d], o2s.at[1 - d, d], o2r.at[1 - d, d], targets[1 - d]))
    for d in range(2):
        remote(far.at[d], r1.at[d], o1s.at[d], o1r.at[d], targets[d]).wait_recv()
        wide = pl.ds(d * 1024, 1024)
        total_out[d] = (part[block_rows(blocks[d]), wide] + r1[d].astype(F32)).astype(BF)
        go(remote(total_out.at[d], r2.at[d, d], o2s.at[d, d], o2r.at[d, d], targets[d]))
    for d in (1, 0):
        for k in (1 - d, d):
            remote(total_out.at[d], r2.at[k, d], o2s.at[k, d], o2r.at[k, d], targets[k]).wait_recv()
        wide = pl.ds(d * 1024, 1024)
        mixed[:, wide] = (part[block_rows(y), wide] + (r2[0, d].astype(F32) + r2[1, d].astype(F32))).astype(BF)
    for copy in sends:
        copy.wait_send()


def on_device(
    tokens, norm_gain, w_glu_a, w_glu_b, conv_taps, ln_gain, w_query, w_key, w_value,
    query_gain, key_gain, lam_head, sub_gain, w_out_conv, w_out_attn,
):
    dma = pltpu.SemaphoreType.DMA

    def vm(*shape, dtype=BF):
        return pltpu.VMEM(shape, dtype)

    return pl.pallas_call(
        layer_kernel,
        out_shape=(jax.ShapeDtypeStruct((64, 2048), BF), jax.ShapeDtypeStruct((2, 4, 256), F32)),
        in_specs=[VM, VM, HBM, HBM, HBM, HBM, HBM, VM, VM, VM, VM, SM, VM, HBM, HBM],
        out_specs=(VM, VM),
        scratch_shapes=[
            vm(4, 64, 2048), vm(256, 2048),
            vm(2048, 512), vm(2048, 512), vm(2048, 512), vm(2048, 128), vm(2048, 128),
            vm(512, 2048), vm(512, 2048),
            vm(256, 512), vm(2, 128, 256), vm(256, 256), vm(256, 256),
            vm(2, 2, NX, NZ, 128, 256), vm(256, 256), vm(2, 4, 256, 128),
            vm(2, 4, 256, 128, dtype=F32), vm(2, 4, 256, 128, dtype=F32), vm(2, 4, 256, 128, dtype=F32),
            vm(32, 512), vm(4, 288, 128, dtype=F32), vm(4, 256, 128, dtype=F32),
            vm(256, 128, dtype=F32), vm(3, 256, 128, dtype=F32),
            vm(256, 256), vm(256, 512), vm(256, 256), vm(256, 256),
            vm(8, 256, dtype=F32), vm(8, 256, dtype=F32), vm(8, 256, dtype=F32),
            vm(256, 2048, dtype=F32), vm(2, 64, 1024), vm(2, 64, 1024), vm(2, 64, 1024), vm(2, 64, 1024),
            vm(2, 2, 64, 1024),
            dma((7,)), dma, dma((2, 2)), dma((2, 2)), dma((2,)), dma((2,)),
            dma((2,)),
            dma((2, 2)), dma((2, 2)),
            dma((4, 2, 2)), dma((4, 2, 2)),
            dma((4, 2, 2)), dma((4, 2, 2)),
            dma((2, 5, 2, 2)), dma((2, 5, 2, 2)),
            dma((2, 5, 2)), dma((2, 5, 2)),
            dma((4,)), dma((4,)),
            dma((3,)), dma((3,)),
            dma((2,)), dma((2,)), dma((2, 2)), dma((2, 2)),
        ],
        compiler_params=pltpu.CompilerParams(
            collective_id=0, has_side_effects=True, vmem_limit_bytes=60 * 1024 * 1024
        ),
        name="layer",
    )(
        tokens, norm_gain.reshape(1, -1), w_glu_a, w_glu_b, w_query, w_key, w_value, query_gain, key_gain,
        conv_taps, ln_gain.reshape(1, -1), lam_head, sub_gain.reshape(1, -1), w_out_conv, w_out_attn,
    )


def solution(mesh):
    return jax.shard_map(
        on_device,
        mesh=mesh,
        in_specs=(
            P(("sp", "tp"), None), P(), P(None, "tp"), P(None, "tp"), P(None, "tp"), P("tp"),
            P(None, "tp"), P(None, "tp"), P(None, "tp"), P("tp", None), P("tp", None), P("tp"),
            P(), P("tp", None), P("tp", None),
        ),
        out_specs=(P(("sp", "tp"), None), P(None, "tp", "sp")),
        check_vma=False,
    )
```

time: 132 us -> 102 us (0.77)
  Pallas kernels: 118 us -> 97.4 us
  local copies, waits for them, and re-layouts: 12.7 us -> 2.96 us
    pallas_call x3 -> x1, Pallas kernels: 118 us -> 97.4 us  [on_device(): pl.pallas_call(layer_kernel, out_shape=(jax.ShapeDtypeStruct((64, 2048),...]
    unnamed x28 -> x2, local copies, waits for them, and re-layouts: 11.1 us -> 2.96 us
where the time goes in v2:
time: 102 us; the launch traced here: 101 us
  Pallas kernels  97.4 us (95%)
  local copies, waits for them, and re-layouts  2.96 us (3%)
    pallas_call x1, Pallas kernels, on_device(): pl.pallas_call(layer_kernel, out_shape=(jax.ShapeDtypeStruct((64, 2048),...  97.4 us
    unnamed x2, local copies, waits for them, and re-layouts  2.96 us

profile of v2, /device:TPU:64, one launch (start us, length us, event | category | flops | bytes accessed | tf_op | source)
XLA Modules:
  0.0 101.0 jit_solution(13323966973824902322)
XLA Ops:
  0.6 97.4 %layer.1 = (bf16[64,2048]{1,0:T(8,128)(2,1)}, f32[2,4,256]{2,1,0:T(4,128)}) custom-call(bf16[64,2048]{1,0:T(8,128)(2,1)} %tok.1, f32[1,2048]{1,0:T(1,128)} %bitcast.3, bf16[2048,512]{1,0:T(8,128)(2,1)} %wa_h.1, bf16[2048,512]{1,0:T(8,128)(2,1)} %wb_h.1, bf16[2048,512]{1,0:T(8,128)(2,1)} %wq_h.1, bf16[2048,128]{1,0:T(8,128)(2,1)} %wk_h.1, ...), custom_call_target="tpu_custom_call" | custom-call | tf_op jit(solution)/shard_map/layer/pallas_call | solution.py:463
  98.1 1.7 %copy.19 = bf16[64,2048]{1,0:T(8,128)(2,1)} copy(bf16[64,2048]{1,0:T(8,128)(2,1)} %get-tuple-element.4) | data formatting | bytes 524288
  99.7 1.3 %copy.20 = f32[2,4,256]{2,1,0:T(4,128)} copy(f32[2,4,256]{2,1,0:T(4,128)} %get-tuple-element.5) | data formatting | bytes 16384

commit v3 on v2

--- a/solution.py
+++ b/solution.py
@@ -43,12 +43,12 @@
 def layer_kernel(
     tok, gain, wa_h, wb_h, wq_h, wk_h, wv_h, qg, kg, taps, ln_gain, lam, sub_gain, wc_h, wo_h,
     mixed, logs,
-    rows, normed, wa, wb, wq, wk, wv, wc, wo, gated, kv_in, q_own, q_far,
+    rows, normed, wa, wb, wq, wk, wv, wc, wo, gated, q_own, q_far,
     kv, q_in, qpad, m_ref, l_ref, acc, halo, gpad, csum, stat_out, stat_in,
     attn, conv_out, ret_out, ret_in, log_out, log_in, log_self,
     part, far, near, total_out, r1, r2,
     w_sem, own_sem, y1s, y1r, y2s, y2r,
-    lc, ax_s, ax_r, az_s, az_r, bz_s, bz_r, bx_s, bx_r, dd_s, dd_r, ex_s, ex_r, st_s, st_r,
+    ax_s, ax_r, az_s, az_r, bz_s, bz_r, bx_s, bx_r, dd_s, dd_r, ex_s, ex_r, st_s, st_r,
     o1s, o1r, o2s, o2r,
 ):
     sp, y = lax.axis_index("sp"), lax.axis_index("tp")
@@ -86,107 +86,143 @@
     def signs(s):
         return (0, 1) if 0 < s < 4 else (0,)
 
-    def hop_halves(s, d):
-        return (0, 1) if s < 4 else (d,)
-
-    def ax1(d):
-        ox = x if d is None else xm(x - 1 + 2 * d)
-        return kv.at[c, 0, ox, z]
-
-    def az(s, d, xh, landing):
-        return kv.at[c, 0, pl.ds(xh * 2, 2), origin(s if landing else s - 1, d)]
-
-    def bz(s, d, rh, landing):
-        return kv.at[c, 1, x, origin(s if landing else s - 1, d), pl.ds(rh * 64, 64)]
-
-    def az_send(s, xh):
-        for d in range(2):
-            if xh in hop_halves(s, d):
-                ref = az(s, d, xh, False)
-                go(remote(ref, ref, az_s.at[s - 1, d, xh], az_r.at[s - 1, d, xh], zdev[d]))
-
-    def az_recv(s, xh):
-        for d in range(2):
-            if xh in hop_halves(s, d):
-                ref = az(s, d, xh, True)
-                remote(ref, ref, az_s.at[s - 1, d, xh], az_r.at[s - 1, d, xh], zdev[d]).wait_recv()
-
-    def bz_send(s):
-        for d in range(2):
-            for rh in hop_halves(s, d):
-                ref = bz(s, d, rh, False)
-                src = kv_in.at[1, pl.ds(rh * 64, 64)] if s == 1 else ref
-                go(remote(src, ref, bz_s.at[s - 1, d, rh], bz_r.at[s - 1, d, rh], zdev[d]))
-
-    def bz_recv(s):
-        for d in range(2):
-            for rh in hop_halves(s, d):
-                ref = bz(s, d, rh, True)
-                remote(ref, ref, bz_s.at[s - 1, d, rh], bz_r.at[s - 1, d, rh], zdev[d]).wait_recv()
-
-    def bx1_send(s):
-        for g in signs(s):
-            ref = kv.at[c, 1, x, origin(s, g)]
+    def ways(s, i):
+        return (0, 1) if s < 4 else (i,)
+
+    offsets = (0, -1, 1, 2)
+
+    def ax1(a, d, landing):
+        ref = kv.at[c, a, xm(x - 1 + 2 * d) if landing else x, z]
+        return remote(ref, ref, ax_s.at[0, a, d], ax_r.at[0, a, d], xdev[d])
+
+    def ax2(a, landing):
+        ref = kv.at[c, a, xm(x + 2) if landing else xm(x - 1 + 2 * a), z]
+        return remote(ref, ref, ax_s.at[1, a, 0], ax_r.at[1, a, 0], xdev[a])
+
+    def az(a, s, d, j, landing):
+        ref = kv.at[c, a, xm(x + offsets[j]), origin(s if landing else s - 1, d)]
+        return remote(ref, ref, az_s.at[a, s - 1, d, j], az_r.at[a, s - 1, d, j], zdev[d])
+
+    def bz(i, s, d, landing):
+        ref = kv.at[c, 2 + i, x, origin(s if landing else s - 1, d)]
+        return remote(ref, ref, bz_s.at[i, s - 1, d], bz_r.at[i, s - 1, d], zdev[d])
+
+    def bx1(i, s, g, d, landing):
+        ref = kv.at[c, 2 + i, xm(x - 1 + 2 * d) if landing else x, origin(s, g)]
+        return remote(ref, ref, bx_s.at[i, s, g, d], bx_r.at[i, s, g, d], xdev[d])
+
+    def bx2(i, s, g, landing):
+        ref = kv.at[c, 2 + i, xm(x + 2) if landing else xm(x - 1 + 2 * i), origin(s, g)]
+        return remote(ref, ref, bx_s.at[i, s, g, 2], bx_r.at[i, s, g, 2], xdev[i])
+
+    def dd(h, s, g, landing):
+        ref = kv.at[sib if landing else c, pl.ds(2 * h, 2), :, origin(s, g)]
+        return remote(ref, ref, dd_s.at[h, s, g], dd_r.at[h, s, g], sdev)
+
+    def a_begin(a):
+        for d in range(2):
+            go(ax1(a, d, False))
+        for d in range(2):
+            go(az(a, 1, d, 0, False))
+
+    def a_x1(a):
+        for d in range(2):
+            ax1(a, d, True).wait_recv()
+        go(ax2(a, False))
+        for j in (1, 2):
             for d in range(2):
-                go(remote(kv_in.at[1] if s == 0 else ref, ref, bx_s.at[0, s, g, d], bx_r.at[0, s, g, d], xdev[d]))
-
-    def bx1_recv(s):
+                go(az(a, 1, d, j, False))
+
+    def a_x2(a):
+        ax2(a, True).wait_recv()
+        for d in range(2):
+            go(az(a, 1, d, 3, False))
+
+    def a_z(a, s):
+        for j in range(4):
+            for d in ways(s, a):
+                az(a, s, d, j, True).wait_recv()
+                if s < 3 or (s == 3 and d == a):
+                    go(az(a, s + 1, d, j, False))
+
+    def b_begin(i):
+        for d in range(2):
+            go(bz(i, 1, d, False))
+        for d in range(2):
+            go(bx1(i, 0, 0, d, False))
+
+    def b_z(i, s):
+        for d in ways(s, i):
+            bz(i, s, d, True).wait_recv()
+            if s < 3 or (s == 3 and d == i):
+                go(bz(i, s + 1, d, False))
+            for way in range(2):
+                go(bx1(i, s, d if s < 4 else 0, way, False))
+
+    def b_x1(i, s):
         for g in signs(s):
             for d in range(2):
-                ref = kv.at[c, 1, xm(x - 1 + 2 * d), origin(s, g)]
-                remote(ref, ref, bx_s.at[0, s, g, d], bx_r.at[0, s, g, d], xdev[d]).wait_recv()
-
-    def bx2_send(s):
+                bx1(i, s, g, d, True).wait_recv()
+            go(bx2(i, s, g, False))
+
+    def b_x2(i, s):
         for g in signs(s):
-            for d in range(2):
-                ref = kv.at[c, 1, xm(x - 1 + 2 * d), origin(s, g), pl.ds(d * 64, 64)]
-                go(remote(ref, ref, bx_s.at[1, s, g, d], bx_r.at[1, s, g, d], xdev[d]))
-
-    def bx2_recv(s):
-        for g in signs(s):
-            for d in range(2):
-                ref = kv.at[c, 1, xm(x + 2), origin(s, g), pl.ds(d * 64, 64)]
-                remote(ref, ref, bx_s.at[1, s, g, d], bx_r.at[1, s, g, d], xdev[d]).wait_recv()
+            bx2(i, s, g, True).wait_recv()
 
     def dd_send(h, s):
         for g in signs(s):
-            ref = kv.at[c, h, :, origin(s, g)]
-            go(remote(ref, ref, dd_s.at[h, s, g], dd_r.at[h, s, g], sdev))
-
-    def dd_recv(h, s):
-        for g in signs(s):
-            ref = kv.at[sib, h, :, origin(s, g)]
-            remote(ref, ref, dd_s.at[h, s, g], dd_r.at[h, s, g], sdev).wait_recv()
+            go(dd(h, s, g, False))
+
+    def dd_recv(s):
+        for h in range(2):
+            for g in signs(s):
+                dd(h, s, g, True).wait_recv()
+
+    slot_rows = [lax.rem(y + k, NT) for k in (0, 3, 1, 2)]
 
     def tile(which, cc, zt, masked):
-        pieces = [(h, k) for h in range(2) for k in range(NX)]
-        keys = jnp.concatenate([kv[cc, h, k, zt, :, 0:128] for h, k in pieces], axis=1)
-        values = jnp.concatenate([kv[cc, h, k, zt, :, 128:256] for h, k in pieces], axis=0)
+        pieces = [(j, k) for j in range(4) for k in range(NX)]
+        keys = jnp.concatenate([kv[cc, j, k, zt, :, 0:128] for j, k in pieces], axis=0)
+        values = jnp.concatenate([kv[cc, j, k, zt, :, 128:256] for j, k in pieces], axis=0)
         if masked:
             row = lax.broadcasted_iota(jnp.int32, (256, 128), 0) + (x * 512 + c * 256)
-            col = lax.broadcasted_iota(jnp.int32, (256, 128), 1) + cc * 256
-        scores = jnp.dot(qpad[which].reshape(1024, 128), keys, preferred_element_type=F32)
-        weights, fades = [], []
-        for hm in range(4):
-            parts = [scores[hm * 256 : (hm + 1) * 256, k * 128 : (k + 1) * 128] for k in range(8)]
-            if masked:
-                parts = [
-                    jnp.where(col + (h * 128 + k * 512) <= row, item, -1e30)
-                    for item, (h, k) in zip(parts, pieces)
-                ]
-            old = m_ref[which, hm]
-            new = jnp.maximum(old, jnp.max(functools.reduce(jnp.maximum, parts), axis=1, keepdims=True))
-            fade = jnp.exp(old - new)
-            parts = [jnp.exp(item - new) for item in parts]
-            m_ref[which, hm] = new
-            l_ref[which, hm] = l_ref[which, hm] * fade + functools.reduce(jnp.add, parts)
-            weights.append(jnp.concatenate([item.astype(BF) for item in parts], axis=1))
-            fades.append(fade)
-        outs = jnp.dot(jnp.concatenate(weights, axis=0), values, preferred_element_type=F32)
-        for hm in range(4):
-            acc[which, hm] = acc[which, hm] * fades[hm] + outs[hm * 256 : (hm + 1) * 256]
-
-    def attend(s, g, cores):
+            col = lax.broadcasted_iota(jnp.int32, (256, 128), 1)
+            col = jnp.where(col < 64, col, col + 448) + cc * 256
+        scores = [
+            lax.dot_general(
+                qpad[which, pl.ds(2 * n, 2)].reshape(512, 128),
+                keys,
+                (((1,), (1,)), ((), ())),
+                preferred_element_type=F32,
+            )
+            for n in range(2)
+        ]
+        for n in range(2):
+            weights, fades = [], []
+            for k in range(2):
+                hm = 2 * n + k
+                parts = [scores[n][k * 256 : (k + 1) * 256, p * 128 : (p + 1) * 128] for p in range(8)]
+                if masked:
+                    parts = [
+                        jnp.where(col + ((p % 2) * 1024 + slot_rows[p // 2] * 64) <= row, item, -1e30)
+                        for p, item in enumerate(parts)
+                    ]
+                old = m_ref[which, hm]
+                new = jnp.maximum(old, jnp.max(functools.reduce(jnp.maximum, parts), axis=1, keepdims=True))
+                fade = jnp.exp(old - new)
+                parts = [jnp.exp(item - new) for item in parts]
+                m_ref[which, hm] = new
+                l_ref[which, hm] = l_ref[which, hm] * fade + functools.reduce(jnp.add, parts)
+                weights.append(jnp.concatenate([item.astype(BF) for item in parts], axis=1))
+                fades.append(fade)
+            outs = jnp.dot(jnp.concatenate(weights, axis=0), values, preferred_element_type=F32)
+            for k in range(2):
+                hm = 2 * n + k
+                acc[which, hm] = acc[which, hm] * fades[k] + outs[k * 256 : (k + 1) * 256]
+
+    early = z < NZ // 2
+
+    def attend(s, g):
         zt = zm(z - s + 2 * s * g)
 
         def step(i, carry):
@@ -198,7 +234,7 @@
             def _():
                 tile(which, cc, zt, False)
 
-            if s in (0, 1, 3):
+            if s in (1, 3):
 
                 @pl.when(zt == zq)
                 def _():
@@ -206,52 +242,41 @@
 
             return carry
 
-        lax.fori_loop(2 * cores[0], 2 * cores[1], step, 0)
-
-    def stage(e):
-        if 1 <= e <= 4:
-            bz_recv(e)
-            if e < 4:
-                bz_send(e + 1)
-            bx1_send(e)
-        if 0 <= e - 1 <= 4:
-            bx1_recv(e - 1)
-            bx2_send(e - 1)
-        if e == 1:
-            for d in range(2):
-                ref = ax1(d)
-                remote(ref, ref, ax_s.at[0, d], ax_r.at[0, d], xdev[d]).wait_recv()
-                ref = kv.at[c, 0, xm(x - 1 + 2 * d), z, pl.ds(d * 64, 64)]
-                go(remote(ref, ref, ax_s.at[1, d], ax_r.at[1, d], xdev[d]))
-        if e == 2:
-            for d in range(2):
-                ref = kv.at[c, 0, xm(x + 2), z, pl.ds(d * 64, 64)]
-                remote(ref, ref, ax_s.at[1, d], ax_r.at[1, d], xdev[d]).wait_recv()
-            az_send(1, 0)
-            az_send(1, 1)
-            dd_send(0, 0)
-        if 0 <= e - 2 <= 4:
-            bx2_recv(e - 2)
-            dd_send(1, e - 2)
-        if e == 3:
-            attend(0, 0, (0, 1))
-        for xh in range(2):
-            if 3 <= e <= 6:
-                az_recv(e - 2, xh)
-                if e < 6:
-                    az_send(e - 1, xh)
-            if e > 3 and xh == 0:
-                dd_recv(0, e - 3)
-                dd_recv(1, e - 3)
-                attend(e - 3, 0, (0, 2))
-        if 3 <= e <= 6:
-            dd_send(0, e - 2)
-        if e == 3:
-            dd_recv(0, 0)
-            dd_recv(1, 0)
-            attend(0, 0, (1, 2))
-        elif 3 < e < 7:
-            attend(e - 3, 1, (0, 2))
+        lax.fori_loop(0, 4, step, 0)
+
+    def attend_first(cc):
+        @pl.when(early)
+        def _():
+            tile(1, cc, z, False)
+
+        @pl.when(jnp.logical_not(early))
+        def _():
+            tile(0, cc, z, True)
+
+    def attend_last():
+        def step(cc, carry):
+            @pl.when(early)
+            def _():
+                tile(0, cc, z, True)
+
+            return carry
+
+        lax.fori_loop(0, 2, step, 0)
+
+    def events_a(t):
+        if t + 1 <= 4:
+            for i in range(2):
+                b_z(i, t + 1)
+        for i in range(2):
+            b_x1(i, t)
+        a_z(0, t)
+
+    def events_b(t):
+        a_z(1, t)
+        dd_send(0, t)
+        for i in range(2):
+            b_x2(i, t)
+        dd_send(1, t)
 
     pairs = ((wk_h, wk), (wv_h, wv), (wq_h, wq), (wa_h, wa), (wb_h, wb), (wc_h, wc), (wo_h, wo))
     loads = [pltpu.make_async_copy(src, dst, w_sem.at[i]) for i, (src, dst) in enumerate(pairs)]
@@ -276,8 +301,22 @@
         scale = lax.rsqrt(jnp.mean(value * value, axis=1, keepdims=True) + 1e-6)
         normed[pl.ds(pl.multiple_of(slot * 64, 64), 64), :] = (value * scale * gain[...]).astype(BF)
 
-    norm_slot(y)
+    def dot(weight):
+        return jnp.dot(normed[...], weight, preferred_element_type=F32)
+
+    def key_slot(j, slot):
+        at_rows = pl.ds(pl.multiple_of(slot * 64, 64), 64)
+        norm_slot(slot)
+        value = normed[at_rows, :]
+        keys = jnp.dot(value, wk[...], preferred_element_type=F32)
+        kv[c, j, x, z, :, 128:256] = jnp.dot(value, wv[...], preferred_element_type=F32).astype(BF)
+        kv[c, j, x, z, :, 0:128] = half_norm(keys, kg[...])
+
+    for load in loads[:2]:
+        load.wait()
+    key_slot(0, y)
     m_ref[...] = jnp.full(m_ref.shape, -1e30, F32)
+    a_begin(0)
     l_ref[...] = jnp.zeros(l_ref.shape, F32)
     acc[...] = jnp.zeros(acc.shape, F32)
     for d in range(2):
@@ -289,23 +328,20 @@
         target, source = ypair[d]
         ref = piece(source, 1 - d)
         remote(ref, ref, y1s.at[d, 1 - d], y1r.at[d, 1 - d], target).wait_recv()
-        norm_slot(source)
+        key_slot(1 + d, source)
+        if d == 0:
+            a_begin(1)
+            a_x1(0)
+        else:
+            b_begin(0)
+    a_x2(0)
     opposite = lax.rem(y + 2, NT)
     for d in range(2):
         ref = piece(opposite, d)
         remote(ref, ref, y2s.at[d], y2r.at[d], ypair[d][0]).wait_recv()
-    norm_slot(opposite)
-
-    def dot(weight):
-        return jnp.dot(normed[...], weight, preferred_element_type=F32)
-
-    for load in loads[:3]:
-        load.wait()
-    key_value = dot(jnp.concatenate([wk[...], wv[...]], axis=1))
-    keys_all = half_norm(key_value[:, :128], kg[...])
-    for h in range(2):
-        kv_in[h, :, 0:128] = keys_all[h * 128 : (h + 1) * 128].T
-        kv_in[h, :, 128:256] = key_value[h * 128 : (h + 1) * 128, 128:].astype(BF)
+    key_slot(3, opposite)
+    b_begin(1)
+    a_x1(1)
 
     def project_q(n, target):
         queries = dot(wq[:, n * 256 : (n + 1) * 256])
@@ -313,27 +349,26 @@
             one = half_norm(queries[:, k * 128 : (k + 1) * 128], qg[2 * n + k : 2 * n + k + 1, :])
             target[:, k * 128 : (k + 1) * 128] = one * jnp.asarray(0.125, BF)
 
+    for load in loads[2:5]:
+        load.wait()
     project_q(1, q_far)
-    own = [pltpu.make_async_copy(kv_in.at[h], kv.at[c, h, x, z], lc.at[h]) for h in range(2)]
-    for copy in own:
-        copy.start()
-    for d in range(2):
-        go(remote(kv_in.at[0], ax1(None), ax_s.at[0, d], ax_r.at[0, d], xdev[d]))
-    bz_send(1)
-    bx1_send(0)
-    for load in loads[3:5]:
-        load.wait()
+    b_z(0, 1)
+    b_x1(0, 0)
+    a_x2(1)
+    dd_send(0, 0)
     for n in range(2):
         span = slice(n * 256, (n + 1) * 256)
         gated[:, span] = (dot(wa[:, span]) * jax.nn.sigmoid(dot(wb[:, span]))).astype(BF)
     q_copy = remote(q_far, q_in, ex_s.at[0], ex_r.at[0], pdev)
     go(q_copy)
+    b_x1(1, 0)
+    b_x2(0, 0)
+    b_z(1, 1)
     project_q(0, q_own)
     halo_copy = remote(gated.at[pl.ds(224, 32)], halo, ex_s.at[1], ex_r.at[1], nxt)
     go(halo_copy)
-    for copy in own:
-        copy.wait()
-    stage(1)
+    b_x2(1, 0)
+    dd_send(1, 0)
     low = lax.broadcasted_iota(jnp.int32, (256, 128), 1) < 64
 
     def pad(which, source):
@@ -359,9 +394,7 @@
         return one + total, two + total * total
 
     nothing = jnp.zeros((256, 128), F32)
-    one, two = lax.fori_loop(0, 2, conv_step, (nothing, nothing))
-    stage(2)
-    one, two = lax.fori_loop(2, 4, conv_step, (one, two))
+    one, two = lax.fori_loop(0, 4, conv_step, (nothing, nothing))
     lane = lax.broadcasted_iota(jnp.int32, (256, 128), 1)
     stat_out[...] = jnp.where(
         lane == 0, jnp.sum(one, axis=1, keepdims=True), jnp.sum(two, axis=1, keepdims=True)
@@ -370,7 +403,11 @@
     pad(1, q_in)
     for k in range(3):
         go(remote(stat_out, stat_in.at[k], st_s.at[k], st_r.at[k], ydev[k]))
-    stage(3)
+    attend_first(c)
+    events_a(1)
+    dd_recv(0)
+    attend_first(sib)
+    events_b(1)
     for k in range(3):
         remote(stat_out, stat_in.at[k], st_s.at[k], st_r.at[k], ydev[k]).wait_recv()
     total = (stat_out[...] + stat_in[0]) + (stat_in[1] + stat_in[2])
@@ -386,8 +423,14 @@
         span = pl.ds(n * 512, 512)
         part[:, span] = jnp.dot(conv_out[...], wc[:, span], preferred_element_type=F32)
 
-    for e in range(4, 8):
-        stage(e)
+    for t in range(1, 5):
+        if t < 4:
+            events_a(t + 1)
+        dd_recv(t)
+        attend(t, 0)
+        if t < 4:
+            events_b(t + 1)
+            attend(t, 1)
 
     def finish(which, out_ref, log_ref):
         table = jnp.zeros((256, 128), F32)
@@ -410,6 +453,7 @@
     ]
     for copy in back:
         go(copy)
+    attend_last()
     finish(0, attn, log_self)
     for n in range(4):
         span = pl.ds(n * 512, 512)
@@ -469,8 +513,8 @@
             vm(4, 64, 2048), vm(256, 2048),
             vm(2048, 512), vm(2048, 512), vm(2048, 512), vm(2048, 128), vm(2048, 128),
             vm(512, 2048), vm(512, 2048),
-            vm(256, 512), vm(2, 128, 256), vm(256, 256), vm(256, 256),
-            vm(2, 2, NX, NZ, 128, 256), vm(256, 256), vm(2, 4, 256, 128),
+            vm(256, 512), vm(256, 256), vm(256, 256),
+            vm(2, 4, NX, NZ, 64, 256), vm(256, 256), vm(2, 4, 256, 128),
             vm(2, 4, 256, 128, dtype=F32), vm(2, 4, 256, 128, dtype=F32), vm(2, 4, 256, 128, dtype=F32),
             vm(32, 512), vm(4, 288, 128, dtype=F32), vm(4, 256, 128, dtype=F32),
             vm(256, 128, dtype=F32), vm(3, 256, 128, dtype=F32),
@@ -479,11 +523,10 @@
             vm(256, 2048, dtype=F32), vm(2, 64, 1024), vm(2, 64, 1024), vm(2, 64, 1024), vm(2, 64, 1024),
             vm(2, 2, 64, 1024),
             dma((7,)), dma, dma((2, 2)), dma((2, 2)), dma((2,)), dma((2,)),
-            dma((2,)),
-            dma((2, 2)), dma((2, 2)),
-            dma((4, 2, 2)), dma((4, 2, 2)),
-            dma((4, 2, 2)), dma((4, 2, 2)),
-            dma((2, 5, 2, 2)), dma((2, 5, 2, 2)),
+            dma((2, 2, 2)), dma((2, 2, 2)),
+            dma((2, 4, 2, 4)), dma((2, 4, 2, 4)),
+            dma((2, 4, 2)), dma((2, 4, 2)),
+            dma((2, 5, 2, 3)), dma((2, 5, 2, 3)),
             dma((2, 5, 2)), dma((2, 5, 2)),
             dma((4,)), dma((4,)),
             dma((3,)), dma((3,)),

time: 102 us -> 99.2 us (0.973)
  Pallas kernels: 97.4 us -> 95.1 us
    pallas_call x1, Pallas kernels: 97.4 us -> 95.1 us  [on_device(): pl.pallas_call(layer_kernel, out_shape=(jax.ShapeDtypeStruct((64, 2048),...]
where the time goes in v3:
time: 99.2 us; the launch traced here: 98.7 us
  Pallas kernels  95.1 us (96%)
  local copies, waits for them, and re-layouts  2.96 us (3%)
    pallas_call x1, Pallas kernels, on_device(): pl.pallas_call(layer_kernel, out_shape=(jax.ShapeDtypeStruct((64, 2048),...  95.1 us
    unnamed x2, local copies, waits for them, and re-layouts  2.96 us

profile of v3, /device:TPU:64, one launch (start us, length us, event | category | flops | bytes accessed | tf_op | source)
XLA Modules:
  0.0 98.7 jit_solution(7212052650284081096)
XLA Ops:
  0.6 95.1 %layer.1 = (bf16[64,2048]{1,0:T(8,128)(2,1)}, f32[2,4,256]{2,1,0:T(4,128)}) custom-call(bf16[64,2048]{1,0:T(8,128)(2,1)} %tok.1, f32[1,2048]{1,0:T(1,128)} %bitcast.3, bf16[2048,512]{1,0:T(8,128)(2,1)} %wa_h.1, bf16[2048,512]{1,0:T(8,128)(2,1)} %wb_h.1, bf16[2048,512]{1,0:T(8,128)(2,1)} %wq_h.1, bf16[2048,128]{1,0:T(8,128)(2,1)} %wk_h.1, ...), custom_call_target="tpu_custom_call" | custom-call | tf_op jit(solution)/shard_map/layer/pallas_call | solution.py:507
  95.7 1.7 %copy.19 = bf16[64,2048]{1,0:T(8,128)(2,1)} copy(bf16[64,2048]{1,0:T(8,128)(2,1)} %get-tuple-element.4) | data formatting | bytes 524288
  97.4 1.3 %copy.20 = f32[2,4,256]{2,1,0:T(4,128)} copy(f32[2,4,256]{2,1,0:T(4,128)} %get-tuple-element.5) | data formatting | bytes 16384

commit v4 on v3

--- a/solution.py
+++ b/solution.py
@@ -76,9 +76,10 @@
     meet = greet([*zdev, *xdev, sdev, pdev, nxt, prv, *ydev])
     sends = []
 
-    def go(copy):
+    def go(copy, keep=True):
         copy.start()
-        sends.append(copy)
+        if keep:
+            sends.append(copy)
 
     def origin(s, d):
         return zm(z - s) if d == 0 else zm(z + s)
@@ -91,79 +92,75 @@
 
     offsets = (0, -1, 1, 2)
 
-    def ax1(a, d, landing):
-        ref = kv.at[c, a, xm(x - 1 + 2 * d) if landing else x, z]
-        return remote(ref, ref, ax_s.at[0, a, d], ax_r.at[0, a, d], xdev[d])
-
-    def ax2(a, landing):
-        ref = kv.at[c, a, xm(x + 2) if landing else xm(x - 1 + 2 * a), z]
-        return remote(ref, ref, ax_s.at[1, a, 0], ax_r.at[1, a, 0], xdev[a])
-
-    def az(a, s, d, j, landing):
-        ref = kv.at[c, a, xm(x + offsets[j]), origin(s if landing else s - 1, d)]
-        return remote(ref, ref, az_s.at[a, s - 1, d, j], az_r.at[a, s - 1, d, j], zdev[d])
+    def ax1(a, d):
+        ref = kv.at[c, a, x, z]
+        go(remote(ref, ref, ax_s, ax_r.at[a, 0], xdev[d]), False)
+
+    def ax2(a):
+        ref = kv.at[c, a, xm(x - 1 + 2 * a), z]
+        go(remote(ref, ref, ax_s, ax_r.at[a, 1], xdev[a]), False)
+
+    def az(a, s, d, j):
+        ref = kv.at[c, a, xm(x + offsets[j]) if s == 1 else slice(None), origin(s - 1, d)]
+        go(remote(ref, ref, az_s, az_r.at[a, s - 1, d], zdev[d]), False)
 
     def bz(i, s, d, landing):
         ref = kv.at[c, 2 + i, x, origin(s if landing else s - 1, d)]
-        return remote(ref, ref, bz_s.at[i, s - 1, d], bz_r.at[i, s - 1, d], zdev[d])
-
-    def bx1(i, s, g, d, landing):
-        ref = kv.at[c, 2 + i, xm(x - 1 + 2 * d) if landing else x, origin(s, g)]
-        return remote(ref, ref, bx_s.at[i, s, g, d], bx_r.at[i, s, g, d], xdev[d])
+        return remote(ref, ref, bz_s, bz_r.at[i, s - 1, d], zdev[d])
+
+    def bx1(i, s, g, d):
+        ref = kv.at[c, 2 + i, x, origin(s, g)]
+        go(remote(ref, ref, bx_s, bx_r.at[i, s, g, 0], xdev[d]), False)
 
     def bx2(i, s, g, landing):
         ref = kv.at[c, 2 + i, xm(x + 2) if landing else xm(x - 1 + 2 * i), origin(s, g)]
-        return remote(ref, ref, bx_s.at[i, s, g, 2], bx_r.at[i, s, g, 2], xdev[i])
-
-    def dd(h, s, g, landing):
-        ref = kv.at[sib if landing else c, pl.ds(2 * h, 2), :, origin(s, g)]
-        return remote(ref, ref, dd_s.at[h, s, g], dd_r.at[h, s, g], sdev)
+        return remote(ref, ref, bx_s, bx_r.at[i, s, g, 1], xdev[i])
+
+    def taken(ref, send, recv):
+        remote(ref, ref, send, recv, sdev).wait_recv()
 
     def a_begin(a):
         for d in range(2):
-            go(ax1(a, d, False))
+            ax1(a, d)
         for d in range(2):
-            go(az(a, 1, d, 0, False))
+            az(a, 1, d, 0)
 
     def a_x1(a):
-        for d in range(2):
-            ax1(a, d, True).wait_recv()
-        go(ax2(a, False))
+        taken(kv.at[c, a, pl.ds(0, 2), z], ax_s, ax_r.at[a, 0])
+        ax2(a)
         for j in (1, 2):
             for d in range(2):
-                go(az(a, 1, d, j, False))
+                az(a, 1, d, j)
 
     def a_x2(a):
-        ax2(a, True).wait_recv()
+        taken(kv.at[c, a, 0, z], ax_s, ax_r.at[a, 1])
         for d in range(2):
-            go(az(a, 1, d, 3, False))
+            az(a, 1, d, 3)
 
     def a_z(a, s):
-        for j in range(4):
-            for d in ways(s, a):
-                az(a, s, d, j, True).wait_recv()
-                if s < 3 or (s == 3 and d == a):
-                    go(az(a, s + 1, d, j, False))
+        for d in ways(s, a):
+            taken(kv.at[c, a, :, origin(s, d)], az_s, az_r.at[a, s - 1, d])
+            if s < 3 or (s == 3 and d == a):
+                az(a, s + 1, d, 0)
 
     def b_begin(i):
         for d in range(2):
-            go(bz(i, 1, d, False))
+            go(bz(i, 1, d, False), False)
         for d in range(2):
-            go(bx1(i, 0, 0, d, False))
+            bx1(i, 0, 0, d)
 
     def b_z(i, s):
         for d in ways(s, i):
             bz(i, s, d, True).wait_recv()
             if s < 3 or (s == 3 and d == i):
-                go(bz(i, s + 1, d, False))
+                go(bz(i, s + 1, d, False), False)
             for way in range(2):
-                go(bx1(i, s, d if s < 4 else 0, way, False))
+                bx1(i, s, d if s < 4 else 0, way)
 
     def b_x1(i, s):
         for g in signs(s):
-            for d in range(2):
-                bx1(i, s, g, d, True).wait_recv()
-            go(bx2(i, s, g, False))
+            taken(kv.at[c, 2 + i, pl.ds(0, 2), origin(s, g)], bx_s, bx_r.at[i, s, g, 0])
+            go(bx2(i, s, g, False), False)
 
     def b_x2(i, s):
         for g in signs(s):
@@ -171,12 +168,22 @@
 
     def dd_send(h, s):
         for g in signs(s):
-            go(dd(h, s, g, False))
+            ref = kv.at[c, pl.ds(2 * h, 2), :, origin(s, g)]
+            go(remote(ref, ref, dd_s, dd_r.at[s, g], sdev), False)
 
     def dd_recv(s):
-        for h in range(2):
-            for g in signs(s):
-                dd(h, s, g, True).wait_recv()
+        for g in signs(s):
+            taken(kv.at[sib, :, :, origin(s, g)], dd_s, dd_r.at[s, g])
+
+    def all_sent():
+        for ref, sem in (
+            (kv.at[c, pl.ds(0, 3), pl.ds(0, 2), 0], ax_s),
+            (kv.at[c, pl.ds(0, 2), :, pl.ds(0, 7)], az_s),
+            (kv.at[c, pl.ds(0, 2), 0, pl.ds(0, 7)], bz_s),
+            (kv.at[c, :, :, pl.ds(0, 3)], bx_s),
+            (kv.at[c], dd_s),
+        ):
+            remote(ref, ref, sem, ax_r.at[0, 0], sdev).wait_send()
 
     slot_rows = [lax.rem(y + k, NT) for k in (0, 3, 1, 2)]
 
@@ -222,12 +229,12 @@
 
     early = z < NZ // 2
 
-    def attend(s, g):
+    def attend(s, g, first=0, last=4):
         zt = zm(z - s + 2 * s * g)
 
         def step(i, carry):
-            which = lax.rem(i, 2)
-            cc = lax.rem(c + i // 2, 2)
+            which = 1 - i // 2
+            cc = lax.rem(c + i, 2)
             zq = jnp.where(which == 0, z, far_z)
 
             @pl.when(zt < zq)
@@ -242,7 +249,7 @@
 
             return carry
 
-        lax.fori_loop(0, 4, step, 0)
+        lax.fori_loop(first, last, step, 0)
 
     def attend_first(cc):
         @pl.when(early)
@@ -267,13 +274,14 @@
         if t + 1 <= 4:
             for i in range(2):
                 b_z(i, t + 1)
-        for i in range(2):
-            b_x1(i, t)
         a_z(0, t)
 
     def events_b(t):
         a_z(1, t)
         dd_send(0, t)
+        if t + 1 <= 4:
+            for i in range(2):
+                b_x1(i, t + 1)
         for i in range(2):
             b_x2(i, t)
         dd_send(1, t)
@@ -282,6 +290,8 @@
     loads = [pltpu.make_async_copy(src, dst, w_sem.at[i]) for i, (src, dst) in enumerate(pairs)]
     own_rows = pltpu.make_async_copy(tok, rows.at[y], own_sem)
     own_rows.start()
+    for load in loads[:2]:
+        load.start()
     meet()
 
     def piece(slot, half):
@@ -292,7 +302,7 @@
         for d in range(2):
             half = order if d == 0 else 1 - order
             go(remote(tok.at[pl.ds(half * 32, 32)], piece(y, half), y1s.at[d, half], y1r.at[d, half], ypair[d][0]))
-    for load in loads:
+    for load in loads[2:]:
         load.start()
     own_rows.wait()
 
@@ -334,7 +344,6 @@
             a_x1(0)
         else:
             b_begin(0)
-    a_x2(0)
     opposite = lax.rem(y + 2, NT)
     for d in range(2):
         ref = piece(opposite, d)
@@ -352,23 +361,27 @@
     for load in loads[2:5]:
         load.wait()
     project_q(1, q_far)
+    q_copy = remote(q_far, q_in, ex_s.at[0], ex_r.at[0], pdev)
+    a_x2(0)
     b_z(0, 1)
     b_x1(0, 0)
+    go(q_copy)
+
+    def gate(n):
+        span = slice(n * 256, (n + 1) * 256)
+        gated[:, span] = (dot(wa[:, span]) * jax.nn.sigmoid(dot(wb[:, span]))).astype(BF)
+
+    gate(0)
     a_x2(1)
     dd_send(0, 0)
-    for n in range(2):
-        span = slice(n * 256, (n + 1) * 256)
-        gated[:, span] = (dot(wa[:, span]) * jax.nn.sigmoid(dot(wb[:, span]))).astype(BF)
-    q_copy = remote(q_far, q_in, ex_s.at[0], ex_r.at[0], pdev)
-    go(q_copy)
+    gate(1)
+    halo_copy = remote(gated.at[pl.ds(224, 32)], halo, ex_s.at[1], ex_r.at[1], nxt)
+    b_z(1, 1)
     b_x1(1, 0)
+    go(halo_copy)
+    project_q(0, q_own)
     b_x2(0, 0)
-    b_z(1, 1)
-    project_q(0, q_own)
-    halo_copy = remote(gated.at[pl.ds(224, 32)], halo, ex_s.at[1], ex_r.at[1], nxt)
-    go(halo_copy)
-    b_x2(1, 0)
-    dd_send(1, 0)
+    b_x1(0, 1)
     low = lax.broadcasted_iota(jnp.int32, (256, 128), 1) < 64
 
     def pad(which, source):
@@ -380,6 +393,8 @@
     pad(0, q_own)
     for k in range(4):
         gpad[k, 32:288, :] = gated[:, k * 128 : (k + 1) * 128].astype(F32)
+    b_x2(1, 0)
+    dd_send(1, 0)
     halo_copy.wait_recv()
     for k in range(4):
         gpad[k, 0:32, :] = jnp.where(sp > 0, halo[:, k * 128 : (k + 1) * 128].astype(F32), 0.0)
@@ -399,6 +414,7 @@
     stat_out[...] = jnp.where(
         lane == 0, jnp.sum(one, axis=1, keepdims=True), jnp.sum(two, axis=1, keepdims=True)
     )
+    b_x1(1, 1)
     q_copy.wait_recv()
     pad(1, q_in)
     for k in range(3):
@@ -423,15 +439,6 @@
         span = pl.ds(n * 512, 512)
         part[:, span] = jnp.dot(conv_out[...], wc[:, span], preferred_element_type=F32)
 
-    for t in range(1, 5):
-        if t < 4:
-            events_a(t + 1)
-        dd_recv(t)
-        attend(t, 0)
-        if t < 4:
-            events_b(t + 1)
-            attend(t, 1)
-
     def finish(which, out_ref, log_ref):
         table = jnp.zeros((256, 128), F32)
         for k in range(2):
@@ -446,13 +453,30 @@
             out_ref[:, k * 128 : (k + 1) * 128] = (diff * scale * sub_gain[...]).astype(BF)
         log_ref[...] = table.T[0:8, :]
 
-    finish(1, ret_out, log_out)
     back = [
         remote(ret_out, ret_in, ex_s.at[2], ex_r.at[2], pdev),
         remote(log_out, log_in, ex_s.at[3], ex_r.at[3], pdev),
     ]
-    for copy in back:
-        go(copy)
+
+    def send_back(now):
+        @pl.when(now)
+        def _():
+            finish(1, ret_out, log_out)
+            for copy in back:
+                copy.start()
+
+    done_by_three = lax.rem(z, 4) >= 2
+    for t in range(1, 4):
+        events_a(t + 1)
+        dd_recv(t)
+        attend(t, 0)
+        events_b(t + 1)
+        attend(t, 1)
+    send_back(done_by_three)
+    dd_recv(4)
+    attend(4, 0, 0, 2)
+    send_back(jnp.logical_not(done_by_three))
+    attend(4, 0, 2, 4)
     attend_last()
     finish(0, attn, log_self)
     for n in range(4):
@@ -491,8 +515,9 @@
             remote(total_out.at[d], r2.at[k, d], o2s.at[k, d], o2r.at[k, d], targets[k]).wait_recv()
         wide = pl.ds(d * 1024, 1024)
         mixed[:, wide] = (part[block_rows(y), wide] + (r2[0, d].astype(F32) + r2[1, d].astype(F32))).astype(BF)
-    for copy in sends:
+    for copy in [*sends, *back]:
         copy.wait_send()
+    all_sent()
 
 
 def on_device(
@@ -523,11 +548,11 @@
             vm(256, 2048, dtype=F32), vm(2, 64, 1024), vm(2, 64, 1024), vm(2, 64, 1024), vm(2, 64, 1024),
             vm(2, 2, 64, 1024),
             dma((7,)), dma, dma((2, 2)), dma((2, 2)), dma((2,)), dma((2,)),
-            dma((2, 2, 2)), dma((2, 2, 2)),
-            dma((2, 4, 2, 4)), dma((2, 4, 2, 4)),
-            dma((2, 4, 2)), dma((2, 4, 2)),
-            dma((2, 5, 2, 3)), dma((2, 5, 2, 3)),
-            dma((2, 5, 2)), dma((2, 5, 2)),
+            dma, dma((2, 2)),
+            dma, dma((2, 4, 2)),
+            dma, dma((2, 4, 2)),
+            dma, dma((2, 5, 2, 2)),
+            dma, dma((5, 2)),
             dma((4,)), dma((4,)),
             dma((3,)), dma((3,)),
             dma((2,)), dma((2,)), dma((2, 2)), dma((2, 2)),

time: 99.2 us -> 94.2 us (0.950)
  Pallas kernels: 95.1 us -> 89.7 us
    pallas_call x1, Pallas kernels: 95.1 us -> 89.7 us  [on_device(): pl.pallas_call(layer_kernel, out_shape=(jax.ShapeDtypeStruct((64, 2048),...]
where the time goes in v4:
time: 94.2 us; the launch traced here: 93.3 us
  Pallas kernels  89.7 us (95%)
  local copies, waits for them, and re-layouts  2.96 us (3%)
    pallas_call x1, Pallas kernels, on_device(): pl.pallas_call(layer_kernel, out_shape=(jax.ShapeDtypeStruct((64, 2048),...  89.7 us
    unnamed x2, local copies, waits for them, and re-layouts  2.96 us

profile of v4, /device:TPU:64, one launch (start us, length us, event | category | flops | bytes accessed | tf_op | source)
XLA Modules:
  0.0 93.3 jit_solution(13665302569035913838)
XLA Ops:
  0.6 89.7 %layer.1 = (bf16[64,2048]{1,0:T(8,128)(2,1)}, f32[2,4,256]{2,1,0:T(4,128)}) custom-call(bf16[64,2048]{1,0:T(8,128)(2,1)} %tok.1, f32[1,2048]{1,0:T(1,128)} %bitcast.3, bf16[2048,512]{1,0:T(8,128)(2,1)} %wa_h.1, bf16[2048,512]{1,0:T(8,128)(2,1)} %wb_h.1, bf16[2048,512]{1,0:T(8,128)(2,1)} %wq_h.1, bf16[2048,128]{1,0:T(8,128)(2,1)} %wk_h.1, ...), custom_call_target="tpu_custom_call" | custom-call | tf_op jit(solution)/shard_map/layer/pallas_call | solution.py:532
  90.3 1.7 %copy.19 = bf16[64,2048]{1,0:T(8,128)(2,1)} copy(bf16[64,2048]{1,0:T(8,128)(2,1)} %get-tuple-element.4) | data formatting | bytes 524288
  92.0 1.3 %copy.20 = f32[2,4,256]{2,1,0:T(4,128)} copy(f32[2,4,256]{2,1,0:T(4,128)} %get-tuple-element.5) | data formatting | bytes 16384

commit v5 on v4

--- a/solution.py
+++ b/solution.py
@@ -350,7 +350,6 @@
         remote(ref, ref, y2s.at[d], y2r.at[d], ypair[d][0]).wait_recv()
     key_slot(3, opposite)
     b_begin(1)
-    a_x1(1)
 
     def project_q(n, target):
         queries = dot(wq[:, n * 256 : (n + 1) * 256])
@@ -362,24 +361,25 @@
         load.wait()
     project_q(1, q_far)
     q_copy = remote(q_far, q_in, ex_s.at[0], ex_r.at[0], pdev)
+    a_x1(1)
     a_x2(0)
-    b_z(0, 1)
-    b_x1(0, 0)
-    go(q_copy)
 
     def gate(n):
         span = slice(n * 256, (n + 1) * 256)
         gated[:, span] = (dot(wa[:, span]) * jax.nn.sigmoid(dot(wb[:, span]))).astype(BF)
 
     gate(0)
+    go(q_copy)
+    b_z(0, 1)
+    b_x1(0, 0)
+    gate(1)
     a_x2(1)
     dd_send(0, 0)
-    gate(1)
+    project_q(0, q_own)
     halo_copy = remote(gated.at[pl.ds(224, 32)], halo, ex_s.at[1], ex_r.at[1], nxt)
+    go(halo_copy)
     b_z(1, 1)
     b_x1(1, 0)
-    go(halo_copy)
-    project_q(0, q_own)
     b_x2(0, 0)
     b_x1(0, 1)
     low = lax.broadcasted_iota(jnp.int32, (256, 128), 1) < 64
@@ -391,10 +391,17 @@
             qpad[which, 2 * k + 1] = jnp.where(low, 0.0, head).astype(BF)
 
     pad(0, q_own)
+    b_x2(1, 0)
+    dd_send(1, 0)
+    q_copy.wait_recv()
+    pad(1, q_in)
+    attend_first(c)
+    b_x1(1, 1)
+    events_a(1)
+    dd_recv(0)
+    attend_first(sib)
     for k in range(4):
         gpad[k, 32:288, :] = gated[:, k * 128 : (k + 1) * 128].astype(F32)
-    b_x2(1, 0)
-    dd_send(1, 0)
     halo_copy.wait_recv()
     for k in range(4):
         gpad[k, 0:32, :] = jnp.where(sp > 0, halo[:, k * 128 : (k + 1) * 128].astype(F32), 0.0)
@@ -414,30 +421,9 @@
     stat_out[...] = jnp.where(
         lane == 0, jnp.sum(one, axis=1, keepdims=True), jnp.sum(two, axis=1, keepdims=True)
     )
-    b_x1(1, 1)
-    q_copy.wait_recv()
-    pad(1, q_in)
     for k in range(3):
         go(remote(stat_out, stat_in.at[k], st_s.at[k], st_r.at[k], ydev[k]))
-    attend_first(c)
-    events_a(1)
-    dd_recv(0)
-    attend_first(sib)
     events_b(1)
-    for k in range(3):
-        remote(stat_out, stat_in.at[k], st_s.at[k], st_r.at[k], ydev[k]).wait_recv()
-    total = (stat_out[...] + stat_in[0]) + (stat_in[1] + stat_in[2])
-    mean = total[:, 0:1] / (NT * 512)
-    mean_sq = total[:, 1:2] / (NT * 512)
-    scale = lax.rsqrt(mean_sq - mean * mean + 1e-5)
-    for k in range(4):
-        span = slice(k * 128, (k + 1) * 128)
-        conv_out[:, span] = jax.nn.silu((csum[k] - mean) * scale * ln_gain[:, span]).astype(BF)
-    for load in loads[5:]:
-        load.wait()
-    for n in range(4):
-        span = pl.ds(n * 512, 512)
-        part[:, span] = jnp.dot(conv_out[...], wc[:, span], preferred_element_type=F32)
 
     def finish(which, out_ref, log_ref):
         table = jnp.zeros((256, 128), F32)
@@ -466,12 +452,30 @@
                 copy.start()
 
     done_by_three = lax.rem(z, 4) >= 2
+    def close_conv():
+        for k in range(3):
+            remote(stat_out, stat_in.at[k], st_s.at[k], st_r.at[k], ydev[k]).wait_recv()
+        total = (stat_out[...] + stat_in[0]) + (stat_in[1] + stat_in[2])
+        mean = total[:, 0:1] / (NT * 512)
+        mean_sq = total[:, 1:2] / (NT * 512)
+        scale = lax.rsqrt(mean_sq - mean * mean + 1e-5)
+        for k in range(4):
+            span = slice(k * 128, (k + 1) * 128)
+            conv_out[:, span] = jax.nn.silu((csum[k] - mean) * scale * ln_gain[:, span]).astype(BF)
+        for load in loads[5:]:
+            load.wait()
+        for n in range(4):
+            span = pl.ds(n * 512, 512)
+            part[:, span] = jnp.dot(conv_out[...], wc[:, span], preferred_element_type=F32)
+
     for t in range(1, 4):
         events_a(t + 1)
         dd_recv(t)
         attend(t, 0)
         events_b(t + 1)
         attend(t, 1)
+        if t == 1:
+            close_conv()
     send_back(done_by_three)
     dd_recv(4)
     attend(4, 0, 0, 2)

time: 94.2 us -> 92.4 us (0.981)
  Pallas kernels: 89.7 us -> 88.6 us
    pallas_call x1, Pallas kernels: 89.7 us -> 88.6 us  [on_device(): pl.pallas_call(layer_kernel, out_shape=(jax.ShapeDtypeStruct((64, 2048),...]
where the time goes in v5:
time: 92.4 us; the launch traced here: 92.2 us
  Pallas kernels  88.6 us (96%)
  local copies, waits for them, and re-layouts  2.96 us (3%)
    pallas_call x1, Pallas kernels, on_device(): pl.pallas_call(layer_kernel, out_shape=(jax.ShapeDtypeStruct((64, 2048),...  88.6 us
    unnamed x2, local copies, waits for them, and re-layouts  2.96 us

profile of v5, /device:TPU:64, one launch (start us, length us, event | category | flops | bytes accessed | tf_op | source)
XLA Modules:
  0.0 92.2 jit_solution(7817603455887767882)
XLA Ops:
  0.6 88.6 %layer.1 = (bf16[64,2048]{1,0:T(8,128)(2,1)}, f32[2,4,256]{2,1,0:T(4,128)}) custom-call(bf16[64,2048]{1,0:T(8,128)(2,1)} %tok.1, f32[1,2048]{1,0:T(1,128)} %bitcast.3, bf16[2048,512]{1,0:T(8,128)(2,1)} %wa_h.1, bf16[2048,512]{1,0:T(8,128)(2,1)} %wb_h.1, bf16[2048,512]{1,0:T(8,128)(2,1)} %wq_h.1, bf16[2048,128]{1,0:T(8,128)(2,1)} %wk_h.1, ...), custom_call_target="tpu_custom_call" | custom-call | tf_op jit(solution)/shard_map/layer/pallas_call | solution.py:536
  89.2 1.7 %copy.19 = bf16[64,2048]{1,0:T(8,128)(2,1)} copy(bf16[64,2048]{1,0:T(8,128)(2,1)} %get-tuple-element.4) | data formatting | bytes 524288
  90.9 1.3 %copy.20 = f32[2,4,256]{2,1,0:T(4,128)} copy(f32[2,4,256]{2,1,0:T(4,128)} %get-tuple-element.5) | data formatting | bytes 16384

commit v6 on v5

--- a/solution.py
+++ b/solution.py
@@ -562,7 +562,7 @@
             dma((2,)), dma((2,)), dma((2, 2)), dma((2, 2)),
         ],
         compiler_params=pltpu.CompilerParams(
-            collective_id=0, has_side_effects=True, vmem_limit_bytes=60 * 1024 * 1024
+            collective_id=0, has_side_effects=True, vmem_limit_bytes=53 * 1024 * 1024
         ),
         name="layer",
     )(

time: 92.4 us -> 95.2 us (1.030)
  local copies, waits for them, and re-layouts: 2.96 us -> 7.11 us
  Pallas kernels: 88.6 us -> 87.2 us
    unnamed x2 -> x18, local copies, waits for them, and re-layouts: 2.96 us -> 7.11 us
    pallas_call x1, Pallas kernels: 88.6 us -> 87.2 us  [on_device(): pl.pallas_call(layer_kernel, out_shape=(jax.ShapeDtypeStruct((64, 2048),...]
where the time goes in v6:
time: 95.2 us; the launch traced here: 94.9 us
  Pallas kernels  87.2 us (92%)
  local copies, waits for them, and re-layouts  7.11 us (7%)
    pallas_call x1, Pallas kernels, on_device(): pl.pallas_call(layer_kernel, out_shape=(jax.ShapeDtypeStruct((64, 2048),...  87.2 us
    unnamed x18, local copies, waits for them, and re-layouts  7.11 us

profile of v6, /device:TPU:64, one launch (start us, length us, event | category | flops | bytes accessed | tf_op | source)
XLA Modules:
  0.0 94.9 jit_solution(16202132467410053778)
XLA Ops:
  0.6 0.0 copy-start
  0.6 0.9 copy-done
  1.6 0.0 copy-start.1
  1.6 0.8 copy-done.1
  2.4 0.0 copy-start.2
  2.4 0.7 copy-done.2
  3.1 0.0 copy-start.3
  3.1 0.7 copy-done.3
  3.8 0.0 copy-start.4
  3.8 0.7 copy-done.4
  4.5 0.0 copy-start.5
  4.5 0.7 copy-done.5
  5.1 0.0 copy-start.6
  5.1 0.7 copy-done.6
  5.8 0.0 copy-start.7
  5.8 0.7 copy-done.7
  6.5 87.2 %layer.1 = (bf16[64,2048]{1,0:T(8,128)(2,1)S(1)}, f32[2,4,256]{2,1,0:T(4,128)S(1)}) custom-call(bf16[64,2048]{1,0:T(8,128)(2,1)S(1)} %copy-done, f32[1,2048]{1,0:T(1,128)S(1)} %bitcast.3, bf16[2048,512]{1,0:T(8,128)(2,1)} %wa_h.1, bf16[2048,512]{1,0:T(8,128)(2,1)} %wb_h.1, bf16[2048,512]{1,0:T(8,128)(2,1)} %wq_h.1, bf16[2048,128]{1,0:T(8,128)(2,1)} %wk_h.1, ...), custom_call_target="tpu_custom_call" | custom-call | tf_op jit(solution)/shard_map/layer/pallas_call | solution.py:536
  93.6 0.7 copy.19
  94.3 0.6 copy.20
Async XLA Ops:
  0.6 1.0 %copy-start = (bf16[64,2048]{1,0:T(8,128)(2,1)S(1)}, bf16[64,2048]{1,0:T(8,128)(2,1)}, u32[]{:S(2)}) copy-start(bf16[64,2048]{1,0:T(8,128)(2,1)} %tok.1) | copy-start | bytes 786436
  1.6 0.8 copy-start.1
  2.4 0.7 copy-start.2
  3.1 0.7 copy-start.3
  3.8 0.7 copy-start.4
  4.5 0.7 copy-start.5
  5.1 0.7 copy-start.6
  5.8 0.7 copy-start.7
